TPU v7x, 32 devices: a whole 2x2x4 slice. The times are simulated.
32 devices in a mesh: sp: 8 (over z, x), tp: 4 (over y, core).
Axes of the slice: x: 2, y: 2, z: 4, core: 2. Of those that a mesh axis runs over, the one named last changes fastest.
Arguments:
- resid: bfloat16 [2048, 4096], P('sp'), may hold values from -6 to 6
- pool_in: bfloat16 [2048, 1024], P('sp', 'tp'), may hold values from -6 to 6
- pool_mix: bfloat16 [4, 256, 256], P('tp'), may hold values from -0.375 to 0.375
- pool_gain: float32 [1024], P('tp'), may hold values from 0.1 to 1.9
- out_proj: bfloat16 [1024, 4096], P('tp'), may hold values from -0.1875 to 0.1875
- norm_gain: float32 [4096], replicated, may hold values from 0.1 to 1.9
- w_gate: bfloat16 [8, 4096, 1024], P('sp', None, 'tp'), may hold values from -0.09375 to 0.09375
- w_up: bfloat16 [8, 4096, 1024], P('sp', None, 'tp'), may hold values from -0.09375 to 0.09375
- w_down: bfloat16 [8, 1024, 4096], P('sp', 'tp'), may hold values from -0.1875 to 0.1875
- routes: int32 [2048, 2], P('sp'), may hold values from 0 to 7, all different within a row; in each aligned block of 64 rows (0 to 63, 64 to 127, ...) at most 32 rows name the same one
- route_weight: float32 [2048, 2], P('sp'), may hold values from 0.25 to 2.5
Outputs:
- layer_out: bfloat16 [2048, 4096], P(('sp', 'tp'))
Inputs may be any that keep to these rules, and one draw needn't show every extreme that they name: `routes`: in each aligned block of 64 tokens no expert is named by more than 32 of the block's rows, and the two experts of a token differ.
All inputs are finite; a program needn't handle non-finite values.
Results may differ from a plain program's by a relative error of at most 0.015.
Values may be sent and summed in bfloat16 or wider, within the bound.
A program may use at most 128 MiB of HBM per device.

v0:
```python
import functools

import jax
import jax.numpy as jnp
from jax import lax
from jax.experimental import pallas as pl
from jax.experimental.pallas import tpu as pltpu
from jax.sharding import PartitionSpec as P

GROUPS = 4


EPS = 1e-06


def shifted(x, axis, by):
    count = lax.axis_size(axis)
    pairs = [(i, i + by) for i in range(count) if 0 <= i + by < count]
    return lax.ppermute(x, axis, pairs)


def rounded(value):
    return lax.optimization_barrier(value.astype(jnp.bfloat16)).astype(jnp.float32)


def group_diff(pool_in):
    row_count = pool_in.shape[0]
    reach = 2**GROUPS
    before = shifted(pool_in[row_count - reach :], "sp", 1)
    joined = jnp.concatenate([before, pool_in], axis=0).astype(jnp.float32)
    running = jnp.cumsum(joined, axis=0)
    width = jnp.left_shift(jnp.int32(2), lax.axis_index("tp"))
    lagged = lax.dynamic_slice_in_dim(running, reach - width, row_count, 0)
    total = running[reach:] - lagged
    place = lax.axis_index("sp") * row_count + jnp.arange(row_count, dtype=jnp.int32) + 1
    counted = jnp.minimum(place, width).astype(jnp.float32)
    return (total / counted[:, None] - joined[reach:]).astype(jnp.bfloat16)


def normalize(mixed, norm_gain):
    scale = lax.rsqrt(jnp.mean(mixed * mixed, axis=1, keepdims=True) + EPS)
    return (mixed * scale * norm_gain).astype(jnp.bfloat16)


def slot_plan(route_rows, blocks, capacity, experts):
    row_count, choose = route_rows.shape
    flat_routes = route_rows.reshape(blocks, row_count // blocks * choose)
    onehot = (
        flat_routes[:, :, None] == jnp.arange(experts, dtype=jnp.int32)[None, None, :]
    ).astype(jnp.int32)
    earlier = jnp.cumsum(onehot, axis=1) - onehot
    position = jnp.sum(earlier * onehot, axis=2)
    block_ids = jnp.arange(blocks, dtype=jnp.int32)[:, None]
    return (flat_routes * (blocks * capacity) + block_ids * capacity + position).reshape(-1)


def fill_slots(normed, targets, slot_count):
    row_count, width = normed.shape
    slots = jnp.arange(slot_count, dtype=jnp.int32)[:, None, None]
    picks = jnp.sum((targets.reshape(row_count, -1)[None] == slots).astype(jnp.bfloat16), axis=2)
    return jnp.dot(picks, normed, preferred_element_type=jnp.float32).astype(normed.dtype)


def collect(returned, targets, weights):
    row_count, choose = weights.shape
    slots = jnp.arange(returned.shape[0], dtype=jnp.int32)[None, None, :]
    chosen = targets.reshape(row_count, choose)[:, :, None] == slots
    spread = jnp.sum(jnp.where(chosen, weights[:, :, None], 0.0), axis=1)
    head = lax.reduce_precision(spread, 8, 7)
    tail = spread - head
    both = jnp.concatenate([head, tail], axis=0).astype(jnp.bfloat16)
    product = jnp.dot(both, returned, preferred_element_type=jnp.float32)
    return product[:row_count] + product[row_count:]


def expert_part(inputs, w_gate, w_up, w_down):
    gate = jnp.dot(inputs, w_gate[0], preferred_element_type=jnp.float32)
    upper = jnp.dot(inputs, w_up[0], preferred_element_type=jnp.float32)
    hidden = (jax.nn.silu(gate) * upper).astype(jnp.bfloat16)
    return jnp.dot(hidden, w_down[0], preferred_element_type=jnp.float32).astype(jnp.bfloat16)


def xor_of(a, b, n):
    total, bit = 0, 1
    while bit < n:
        total = total + ((a // bit + b // bit) % 2) * bit
        bit *= 2
    return total


def moe_kernel(
    n, slices, capacity,
    outgoing, wg_hbm, wu_hbm, wd_hbm, out,
    wg, wu, wd, rows, parts, pair_in, y_in,
    w_sem, own_sem,
    sp_send, sp_recv, fy_send, fy_recv, fa_send, fa_recv, fb_send, fb_recv,
    pp_send, pp_recv, ry_send, ry_recv, rs_send, rs_recv,
):
    me = lax.axis_index("sp")
    tp = lax.axis_index("tp")
    core, y = tp % 2, tp // 2
    mate = y * 2 + (1 - core)
    across = (1 - y) * 2 + core
    C = capacity

    def spot(c, yy):
        return pl.ds(pl.multiple_of((c * 2 + yy) * C, C), C)

    def half(c):
        return pl.ds(pl.multiple_of(c * 2 * C, 2 * C), 2 * C)

    def offset(j):
        return j

    def chunk(j):
        return xor_of(me, offset(j), n)

    def remote(src, dst, send, recv, to):
        return pltpu.make_async_remote_copy(
            src_ref=src, dst_ref=dst, send_sem=send, recv_sem=recv,
            device_id=to, device_id_type=pl.DeviceIdType.MESH,
        )

    def sp_copy(j):
        s = chunk(j)
        return remote(outgoing.at[s], rows.at[me, spot(core, y)],
                      sp_send.at[j], sp_recv.at[j], (s, tp))

    def fy_copy(j):
        s = chunk(j)
        ref = rows.at[s, spot(core, y)]
        return remote(ref, ref, fy_send.at[j], fy_recv.at[j], (me, across))

    def fa_copy(j):
        s = chunk(j)
        ref = rows.at[s, spot(core, y)]
        return remote(ref, ref, fa_send.at[j], fa_recv.at[j], (me, mate))

    def fb_copy(j):
        s = chunk(j)
        ref = rows.at[s, spot(core, 1 - y)]
        return remote(ref, ref, fb_send.at[j], fb_recv.at[j], (me, mate))

    def pp_copy(j):
        s = chunk(j)
        return remote(parts.at[s, half(1 - core)], pair_in.at[s],
                      pp_send.at[j], pp_recv.at[j], (me, mate))

    def ry_copy(j):
        s = chunk(j)
        return remote(parts.at[s, spot(core, 1 - y)], y_in.at[s],
                      ry_send.at[j], ry_recv.at[j], (me, across))

    def rs_copy(j):
        s = chunk(j)
        return remote(parts.at[s, spot(core, y)], out.at[me],
                      rs_send.at[j], rs_recv.at[j], (s, tp))

    loads = [
        pltpu.make_async_copy(wg_hbm.at[0], wg, w_sem.at[0]),
        pltpu.make_async_copy(wu_hbm.at[0], wu, w_sem.at[1]),
        pltpu.make_async_copy(wd_hbm.at[0], wd, w_sem.at[2]),
    ]
    own = pltpu.make_async_copy(outgoing.at[me], rows.at[me, spot(core, y)], own_sem)
    own.start()

    barrier = pltpu.get_barrier_semaphore()

    @pl.loop(1, n)
    def _(j):
        pl.semaphore_signal(barrier, inc=1, device_id=(xor_of(me, j, n), tp),
                               device_id_type=pl.DeviceIdType.MESH)

    for peer in (mate, across):
        pl.semaphore_signal(barrier, inc=1, device_id=(me, peer),
                               device_id_type=pl.DeviceIdType.MESH)
    pl.semaphore_wait(barrier, n + 1)

    @pl.loop(1, n)
    def _(j):
        sp_copy(j).start()

    for load in loads:
        load.start()

    def compute(s):
        x = rows[s]
        gate = jnp.dot(x, wg[...], preferred_element_type=jnp.float32)
        upper = jnp.dot(x, wu[...], preferred_element_type=jnp.float32)
        hidden = (gate * (1.0 / (1.0 + jnp.exp(-gate))) * upper).astype(jnp.bfloat16)
        width = wd.shape[1]
        tile = min(1024, width)

        @pl.loop(0, width // tile)
        def _(k):
            cols = pl.ds(pl.multiple_of(k * tile, tile), tile)
            parts[s, :, cols] = jnp.dot(
                hidden, wd[:, cols], preferred_element_type=jnp.float32
            ).astype(jnp.bfloat16)

    @pl.loop(0, n + 3)
    def _(j):
        @pl.when(j == 0)
        def _():
            own.wait()

        @pl.when((j >= 1) & (j < n))
        def _():
            sp_copy(j).wait_recv()

        @pl.when(j < n)
        def _():
            fy_copy(j).start()
            fa_copy(j).start()

        @pl.when((j >= 2) & (j < n + 2))
        def _():
            k = j - 2
            s = chunk(k)
            pp_copy(k).wait_recv()
            there = spot(core, 1 - y)
            far = pl.ds(pl.multiple_of((1 - y) * C, C), C)
            parts[s, there] = (
                parts[s, there].astype(jnp.float32) + pair_in[s, far].astype(jnp.float32)
            ).astype(jnp.bfloat16)
            ry_copy(k).start()

        @pl.when(j >= 3)
        def _():
            k = j - 3
            s = chunk(k)
            ry_copy(k).wait_recv()
            here = spot(core, y)
            near = pl.ds(pl.multiple_of(y * C, C), C)
            total = (
                parts[s, here].astype(jnp.float32)
                + pair_in[s, near].astype(jnp.float32)
                + y_in[s].astype(jnp.float32)
            ).astype(jnp.bfloat16)

            @pl.when(k == 0)
            def _():
                out[me] = total

            @pl.when(k > 0)
            def _():
                parts[s, here] = total
                rs_copy(k).start()

        @pl.when((j >= 1) & (j < n + 1))
        def _():
            k = j - 1
            fy_copy(k).wait_recv()
            fb_copy(k).start()

            @pl.when(k == 0)
            def _():
                for load in loads:
                    load.wait()

            fa_copy(k).wait_recv()
            fb_copy(k).wait_recv()
            compute(chunk(k))
            pp_copy(k).start()

    @pl.loop(0, n)
    def _(j):
        fy_copy(j).wait_send()
        fa_copy(j).wait_send()
        fb_copy(j).wait_send()
        pp_copy(j).wait_send()
        ry_copy(j).wait_send()

        @pl.when(j > 0)
        def _():
            sp_copy(j).wait_send()
            rs_copy(j).wait_send()
            rs_copy(j).wait_recv()


def moe_exchange(outgoing, w_gate, w_up, w_down, slices):
    n, capacity, width = outgoing.shape
    units = w_gate.shape[2]
    bf16 = jnp.bfloat16
    dma = pltpu.SemaphoreType.DMA
    return pl.pallas_call(
        functools.partial(moe_kernel, n, slices, capacity),
        out_shape=jax.ShapeDtypeStruct(outgoing.shape, bf16),
        in_specs=[pl.BlockSpec(memory_space=pltpu.VMEM)]
        + [pl.BlockSpec(memory_space=pl.ANY)] * 3,
        out_specs=pl.BlockSpec(memory_space=pltpu.VMEM),
        scratch_shapes=[
            pltpu.VMEM((width, units), bf16),
            pltpu.VMEM((width, units), bf16),
            pltpu.VMEM((units, width), bf16),
            pltpu.VMEM((n, slices * capacity, width), bf16),
            pltpu.VMEM((n, slices * capacity, width), bf16),
            pltpu.VMEM((n, 2 * capacity, width), bf16),
            pltpu.VMEM((n, capacity, width), bf16),
            dma((3,)),
            dma,
        ]
        + [dma((n,))] * 14,
        compiler_params=pltpu.CompilerParams(
            collective_id=1, has_side_effects=True, vmem_limit_bytes=52 * 2**20
        ),
        cost_estimate=pl.CostEstimate(
            flops=6 * n * slices * capacity * width * units,
            bytes_accessed=3 * 2 * width * units,
            transcendentals=0,
        ),
        name="moe_exchange",
    )(outgoing, w_gate, w_up, w_down)


def sum_kernel(count, part, out, pair_in, total, y_in, pp_send, pp_recv, y_send, y_recv):
    me = lax.axis_index("sp")
    tp = lax.axis_index("tp")
    core, y = tp % 2, tp // 2
    mate = y * 2 + (1 - core)
    across = (1 - y) * 2 + core
    pieces = count // 16
    mesh_id = pl.DeviceIdType.MESH
    barrier = pltpu.get_barrier_semaphore()
    for peer in (mate, across):
        pl.semaphore_signal(barrier, inc=1, device_id=(me, peer), device_id_type=mesh_id)
    pl.semaphore_wait(barrier, 2)

    def at(yy, c, k):
        return pl.ds(pl.multiple_of((yy * 2 + c) * count + k * 16, 16), 16)

    def piece(k):
        return pl.ds(pl.multiple_of(k * 16, 16), 16)

    def pair_copy(yy, k, place):
        return pltpu.make_async_remote_copy(
            src_ref=part.at[at(yy, 1 - core, k)], dst_ref=pair_in.at[place, piece(k)],
            send_sem=pp_send.at[place, k], recv_sem=pp_recv.at[place, k],
            device_id=(me, mate), device_id_type=mesh_id,
        )

    def far_copy(k):
        return pltpu.make_async_remote_copy(
            src_ref=total.at[piece(k)], dst_ref=y_in.at[piece(k)],
            send_sem=y_send.at[k], recv_sem=y_recv.at[k],
            device_id=(me, across), device_id_type=mesh_id,
        )

    @pl.loop(0, pieces)
    def _(k):
        pair_copy(1 - y, k, 0).start()

    @pl.loop(0, pieces)
    def _(k):
        pair_copy(y, k, 1).start()

    @pl.loop(0, pieces)
    def _(k):
        pair_copy(1 - y, k, 0).wait_recv()
        total[piece(k)] = (
            part[at(1 - y, core, k)].astype(jnp.float32)
            + pair_in[0, piece(k)].astype(jnp.float32)
        ).astype(jnp.bfloat16)
        far_copy(k).start()

    @pl.loop(0, pieces)
    def _(k):
        pair_copy(y, k, 1).wait_recv()
        far_copy(k).wait_recv()
        out[piece(k)] = (
            part[at(y, core, k)].astype(jnp.float32)
            + pair_in[1, piece(k)].astype(jnp.float32)
            + y_in[piece(k)].astype(jnp.float32)
        ).astype(jnp.bfloat16)

    @pl.loop(0, pieces)
    def _(k):
        pair_copy(1 - y, k, 0).wait_send()
        pair_copy(y, k, 1).wait_send()
        far_copy(k).wait_send()


def scatter_sum(part, slices):
    row_count, width = part.shape
    count = row_count // slices
    pieces = count // 16
    bf16 = jnp.bfloat16
    dma = pltpu.SemaphoreType.DMA
    return pl.pallas_call(
        functools.partial(sum_kernel, count),
        out_shape=jax.ShapeDtypeStruct((count, width), bf16),
        in_specs=[pl.BlockSpec(memory_space=pltpu.VMEM)],
        out_specs=pl.BlockSpec(memory_space=pltpu.VMEM),
        scratch_shapes=[
            pltpu.VMEM((2, count, width), bf16),
            pltpu.VMEM((count, width), bf16),
            pltpu.VMEM((count, width), bf16),
            dma((2, pieces)),
            dma((2, pieces)),
            dma((pieces,)),
            dma((pieces,)),
        ],
        compiler_params=pltpu.CompilerParams(
            collective_id=2, has_side_effects=True, vmem_limit_bytes=24 * 2**20
        ),
        cost_estimate=pl.CostEstimate(flops=0, bytes_accessed=2**25, transcendentals=0),
        name="scatter_sum",
    )(part)


def on_device(
    resid,
    pool_in,
    pool_mix,
    pool_gain,
    out_proj,
    norm_gain,
    w_gate,
    w_up,
    w_down,
    routes,
    route_weight,
):
    token_count, width = resid.shape
    choose = routes.shape[1]
    experts = lax.axis_size("sp")
    slices = lax.axis_size("tp")
    sub_count = token_count // slices
    capacity = max(2, 2 * sub_count * choose // experts)
    tp_index = lax.axis_index("tp")
    diff = group_diff(pool_in)
    pooled = (jnp.dot(diff, pool_mix[0], preferred_element_type=jnp.float32) * pool_gain).astype(
        jnp.bfloat16
    )
    group_part = rounded(jnp.dot(pooled, out_proj, preferred_element_type=jnp.float32)).astype(
        jnp.bfloat16
    )
    if slices == 4 and sub_count % 16 == 0:
        proj = scatter_sum(group_part, slices).astype(jnp.float32)
    else:
        proj = rounded(
            lax.psum_scatter(group_part, "tp", scatter_dimension=0, tiled=True).astype(jnp.float32)
        )
    first = tp_index * sub_count
    mixed = lax.dynamic_slice_in_dim(resid, first, sub_count, 0).astype(jnp.float32) + proj
    normed = normalize(mixed, norm_gain)
    route_rows = lax.dynamic_slice_in_dim(routes, first, sub_count, 0)
    weight_rows = lax.dynamic_slice_in_dim(route_weight, first, sub_count, 0)
    targets = slot_plan(route_rows, 1, capacity, experts)
    outgoing = fill_slots(normed, targets, experts * capacity).reshape(experts, capacity, width)
    if slices == 4 and capacity % 16 == 0 and experts & (experts - 1) == 0:
        returned = moe_exchange(outgoing, w_gate, w_up, w_down, slices)
    else:
        arrived = lax.all_to_all(outgoing, "sp", split_axis=0, concat_axis=0, tiled=True)
        block_rows = lax.all_gather(arrived, "tp", axis=0, tiled=True)
        spread = expert_part(block_rows.reshape(-1, width), w_gate, w_up, w_down).reshape(
            block_rows.shape
        )
        stacked = spread.reshape((slices,) + arrived.shape)
        received = lax.all_to_all(stacked, "tp", split_axis=0, concat_axis=0, tiled=True)
        summed = jnp.sum(received.astype(jnp.float32), axis=0)
        returned = lax.all_to_all(
            summed.astype(jnp.bfloat16), "sp", split_axis=0, concat_axis=0, tiled=True
        )
    moe = collect(returned.reshape(-1, width), targets, weight_rows)
    return (mixed + moe).astype(jnp.bfloat16)


def solution(mesh):
    in_specs = (
        P("sp", None),
        P("sp", "tp"),
        P("tp", None, None),
        P("tp"),
        P("tp", None),
        P(),
        P("sp", None, "tp"),
        P("sp", None, "tp"),
        P("sp", "tp", None),
        P("sp", None),
        P("sp", None),
    )
    out_specs = P(("sp", "tp"), None)
    return jax.shard_map(
        on_device, mesh=mesh, in_specs=in_specs, out_specs=out_specs, check_vma=False
    )
```

profile of v0, /device:TPU:8, one launch (start us, length us, event | category | flops | bytes accessed | tf_op | source)
XLA Modules:
  0.0 159.2 jit_solution(12985339035720144108)
XLA Ops:
  0.0 0.0 copy-start
  0.0 0.8 slice.25
  0.9 3.4 %collective-permute-start = (bf16[16,256]{1,0:T(8,128)(2,1)S(1)}, bf16[16,256]{1,0:T(8,128)(2,1)S(1)}, u32[]{:S(2)}, u32[]{:S(2)}) collective-permute-start(bf16[16,256]{1,0:T(8,128)(2,1)S(1)} %slice.25), channel_id=1, source_target_pairs={{0,4},{4,8},{8,12},{12,16},{16,20},{20,24},{24,28},{1,5},{5,9},{9,... | collective-permute-start | bytes 24584 | tf_op jit(solution)/shard_map/ppermute | solution.py:19
  4.3 0.8 constant_dynamic-slice_fusion
  5.0 0.7 constant_dynamic-slice_fusion.1
  5.8 0.1 copy.26
  5.9 0.1 eq.53
  6.0 0.1 fusion.24
  6.1 0.2 reduce_window_sum.28
  6.3 0.2 select_reduce_fusion.1
  6.4 0.1 reduce_sum.42
  6.6 0.1 copy.27
  6.7 0.8 multiply_add_fusion
  7.4 0.1 fusion.19
  7.5 0.1 select_reduce_fusion
  7.7 0.0 collective-permute-done
  7.7 0.9 fusion.25
  8.6 0.0 copy-start.3
  8.6 0.0 copy-start.5
  8.7 0.3 fusion.3
  9.0 0.1 broadcast_add_fusion
  9.1 0.1 copy.25
  9.2 0.0 copy-done
  9.2 0.3 copy-done.3
  9.5 2.2 %convolution_convert_fusion.1.part = bf16[256,4096]{1,0:T(8,128)(2,1)} fusion(bf16[256,4096]{1,0:T(8,128)(2,1)S(1)} %copy-done, f32[272,256]{1,0:T(8,128)S(1)} %get-tuple-element.6, f32[384,256]{1,0:T(8,128)S(1)} %bitcast.19, f32[272,256]{1,0:T(8,128)S(1)} %slice.36, s32[]{:T(128)S(6)} %select_n.13, bf16[1,256,256]{2,1,0:T(8,128)(2,1)S(1)} %copy-done.3, ...), kind=kOutput, calls=%fused_computation.1 | convolution fusion | flops 571867136 | bytes 5113860 | tf_op jit(solution)/shard_map/dot_general | solution.py:435
  11.8 1.6 copy-done.1
  13.4 15.8 %scatter_sum.1 = bf16[64,4096]{1,0:T(8,128)(2,1)S(1)} custom-call(bf16[256,4096]{1,0:T(8,128)(2,1)S(1)} %copy-done.1), custom_call_target="tpu_custom_call" | custom-call | bytes 33554432 | tf_op jit(solution)/shard_map/scatter_sum/pallas_call | solution.py:389
  29.2 0.3 multiply_reduce_fusion
  29.5 2.1 %convolution_convert_fusion = bf16[256,4096]{1,0:T(8,128)(2,1)} fusion(bf16[256,64]{0,1:T(8,128)(2,1)S(1)} %fusion.19, bf16[64,4096]{1,0:T(8,128)(2,1)S(1)} %scatter_sum.1, f32[4096]{0:T(1024)S(1)} %copy-done.4, f32[64]{0:T(128)S(1)} %add_rsqrt_fusion, bf16[256,4096]{1,0:T(8,128)(2,1)S(1)} %copy-done.2, s32[]{:T(128)S(6)} %select_n.12), kind=kOutput, calls=%fused_computation | convolution fusion | flops 136839168 | bytes 3195396 | tf_op jit(solution)/shard_map/dot_general | solution.py:61
  31.6 124.6 %moe_exchange.1 = bf16[8,32,4096]{2,1,0:T(8,128)(2,1)} custom-call(bf16[8,32,4096]{2,1,0:T(8,128)(2,1)} %bitcast.21, bf16[1,4096,256]{2,1,0:T(8,128)(2,1)} %wg_hbm.1, bf16[1,4096,256]{2,1,0:T(8,128)(2,1)} %wu_hbm.1, bf16[1,256,4096]{2,1,0:T(8,128)(2,1)} %wd_hbm.1), custom_call_target="tpu_custom_call" | custom-call | flops 6442450944 | bytes 6291456 | tf_op jit(solution)/shard_map/moe_exchange/pallas_call | solution.py:286
  156.2 2.0 %fusion.20 = f32[128,4096]{1,0:T(8,128)S(1)} fusion(bf16[256,4096]{1,0:T(8,128)(2,1)} %bitcast.20, bf16[64,256]{1,0:T(8,128)(2,1)S(1)} %get-tuple-element.8, bf16[64,256]{1,0:T(8,128)(2,1)S(1)} %get-tuple-element.7), kind=kOutput, calls=%fused_computation.32 | convolution fusion | flops 268566528 | bytes 4259840 | tf_op jit(solution)/shard_map/dot_general | solution.py:72
  158.2 1.0 fusion.2
  (13 shorter events, 0.1 us)
Async XLA Ops:
  0.0 9.2 %copy-start = (bf16[256,4096]{1,0:T(8,128)(2,1)S(1)}, bf16[256,4096]{1,0:T(8,128)(2,1)}, u32[]{:S(2)}) copy-start(bf16[256,4096]{1,0:T(8,128)(2,1)} %param.15) | copy-start | bytes 6291460
  0.9 6.8 %collective-permute-start = (bf16[16,256]{1,0:T(8,128)(2,1)S(1)}, bf16[16,256]{1,0:T(8,128)(2,1)S(1)}, u32[]{:S(2)}, u32[]{:S(2)}) collective-permute-start(bf16[16,256]{1,0:T(8,128)(2,1)S(1)} %slice.25), channel_id=1, source_target_pairs={{0,4},{4,8},{8,12},{12,16},{16,20},{20,24},{24,28},{1,5},{5,9},{9,... | collective-permute-start | bytes 24584 | tf_op jit(solution)/shard_map/ppermute | solution.py:19
  8.6 0.9 copy-start.3
  8.6 0.9 copy-start.5
  11.8 1.6 copy-start.1
  13.4 15.8 %copy-start.2 = (bf16[256,4096]{1,0:T(8,128)(2,1)S(1)}, bf16[256,4096]{1,0:T(8,128)(2,1)}, u32[]{:S(2)}) copy-start(bf16[256,4096]{1,0:T(8,128)(2,1)} %param.11) | copy-start | bytes 6291460
  13.4 16.1 %copy-start.4 = (f32[4096]{0:T(1024)S(1)}, f32[4096]{0:T(1024)}, u32[]{:S(2)}) copy-start(f32[4096]{0:T(1024)} %param.16) | copy-start | bytes 49156
where the time goes:
time: 160 us; the launch traced here: 159 us
  Pallas kernels  140 us (88%)
  matrix products  6.4 us (4%)
  local copies, waits for them, and re-layouts  4.84 us (3%)
  other arithmetic  4.03 us (3%)
  starting transfers between devices  3.39 us (2%)
    pallas_call x1, Pallas kernels, moe_exchange(): pl.pallas_call(functools.partial(moe_kernel, n, slices, capacity), out_sh...  125 us
    pallas_call x1, Pallas kernels, scatter_sum(): pl.pallas_call(functools.partial(sum_kernel, count), out_shape=jax.ShapeD...  15.8 us
    ppermute x1, starting transfers between devices, shifted(): return lax.ppermute(x, axis, pairs)  3.39 us
  transfers between devices with their start and end apart: 1, of which 0 were waited for; matrix products, arithmetic and copies ran while one was open for 2% of the time, Pallas kernels for 0%

commit v1 on v0

--- a/solution.py
+++ b/solution.py
@@ -80,40 +80,41 @@
     return jnp.dot(hidden, w_down[0], preferred_element_type=jnp.float32).astype(jnp.bfloat16)
 
 
-def xor_of(a, b, n):
-    total, bit = 0, 1
-    while bit < n:
-        total = total + ((a // bit + b // bit) % 2) * bit
-        bit *= 2
-    return total
+def line_plan(z):
+    first = z + 1 - 2 * (z % 2)
+    second = 2 - z // 2
+    third = 3 - 3 * (z // 2)
+    return first, second, third
 
 
 def moe_kernel(
-    n, slices, capacity,
-    outgoing, wg_hbm, wu_hbm, wd_hbm, out,
-    wg, wu, wd, rows, parts, pair_in, y_in,
-    w_sem, own_sem,
-    sp_send, sp_recv, fy_send, fy_recv, fa_send, fa_recv, fb_send, fb_recv,
-    pp_send, pp_recv, ry_send, ry_recv, rs_send, rs_recv,
+    front, back, capacity, experts,
+    rows_in, meta_in, wg_hbm, wu_hbm, wd_hbm, out,
+    wg, wu, wd, rows, meta, slots, give, parts,
+    mate_in, y_in, x_in, sums, line_in, home_in, last_in,
+    w_sem, m_send, m_recv, r_recv, ry_send, ra_send, rb_send,
+    xf_send, xf_recv, yf_send, yf_recv, mf_send, mf_recv,
+    mb_send, mb_recv, yb_send, yb_recv, xb_send, xb_recv,
+    zf_send, zf_recv, zh_send, zh_recv, yl_send, yl_recv,
 ):
     me = lax.axis_index("sp")
     tp = lax.axis_index("tp")
-    core, y = tp % 2, tp // 2
-    mate = y * 2 + (1 - core)
-    across = (1 - y) * 2 + core
+    z, x = me // 2, me % 2
+    y, c = tp // 2, tp % 2
     C = capacity
-
-    def spot(c, yy):
-        return pl.ds(pl.multiple_of((c * 2 + yy) * C, C), C)
-
-    def half(c):
-        return pl.ds(pl.multiple_of(c * 2 * C, 2 * C), 2 * C)
-
-    def offset(j):
-        return j
-
-    def chunk(j):
-        return xor_of(me, offset(j), n)
+    tokens, width = rows_in.shape
+    wf, wb = width // front, width // back
+    z1, z2, z3 = line_plan(z)
+    mid = ((z + 1) // 2) % 2 == 1
+    end = ((z + 1) // 2) % 2 == 0
+    mate = (me, y * 2 + 1 - c)
+    across = (me, (1 - y) * 2 + c)
+    peer_expert = me + 1 - 2 * x
+    beside = (peer_expert, tp)
+    f32, bf16 = jnp.float32, jnp.bfloat16
+
+    def plane(zz):
+        return (zz * 2 + x, tp)
 
     def remote(src, dst, send, recv, to):
         return pltpu.make_async_remote_copy(
@@ -121,196 +122,568 @@
             device_id=to, device_id_type=pl.DeviceIdType.MESH,
         )
 
-    def sp_copy(j):
-        s = chunk(j)
-        return remote(outgoing.at[s], rows.at[me, spot(core, y)],
-                      sp_send.at[j], sp_recv.at[j], (s, tp))
-
-    def fy_copy(j):
-        s = chunk(j)
-        ref = rows.at[s, spot(core, y)]
-        return remote(ref, ref, fy_send.at[j], fy_recv.at[j], (me, across))
-
-    def fa_copy(j):
-        s = chunk(j)
-        ref = rows.at[s, spot(core, y)]
-        return remote(ref, ref, fa_send.at[j], fa_recv.at[j], (me, mate))
-
-    def fb_copy(j):
-        s = chunk(j)
-        ref = rows.at[s, spot(core, 1 - y)]
-        return remote(ref, ref, fb_send.at[j], fb_recv.at[j], (me, mate))
-
-    def pp_copy(j):
-        s = chunk(j)
-        return remote(parts.at[s, half(1 - core)], pair_in.at[s],
-                      pp_send.at[j], pp_recv.at[j], (me, mate))
-
-    def ry_copy(j):
-        s = chunk(j)
-        return remote(parts.at[s, spot(core, 1 - y)], y_in.at[s],
-                      ry_send.at[j], ry_recv.at[j], (me, across))
-
-    def rs_copy(j):
-        s = chunk(j)
-        return remote(parts.at[s, spot(core, y)], out.at[me],
-                      rs_send.at[j], rs_recv.at[j], (s, tp))
+    def fcols(h):
+        return pl.ds(pl.multiple_of(h * wf, wf), wf)
+
+    def bcols(h):
+        return pl.ds(pl.multiple_of(h * wb, wb), wb)
+
+    def spot(xx, yy):
+        return pl.ds(pl.multiple_of(c * 4 * C + xx * 2 * C + yy * C, C), C)
+
+    def both(xx):
+        return pl.ds(pl.multiple_of(c * 4 * C + xx * 2 * C, 2 * C), 2 * C)
+
+    def half(cc):
+        return pl.ds(pl.multiple_of(cc * 4 * C, 4 * C), 4 * C)
+
+    def strip(yy):
+        return pl.ds(pl.multiple_of(yy * C, C), C)
+
+    def meta_copy(q):
+        zq, yq = (z + q // 2) % 4, (y + q) % 2
+        return remote(meta_in, meta.at[z, y], m_send.at[q], m_recv.at[z, y],
+                      (zq * 2 + x, yq * 2 + c))
+
+    def meta_here(zt, yt):
+        remote(meta.at[zt, yt], meta.at[zt, yt], m_send.at[0], m_recv.at[zt, yt],
+               mate).wait_recv()
+
+    def dup_copy(h):
+        return remote(rows_in.at[:, fcols(h)], rows.at[z, y, :, fcols(h)],
+                      ry_send.at[h], r_recv.at[z, y, h], across)
+
+    def own_copy(h, to, send):
+        return remote(rows_in.at[:, fcols(h)], rows.at[z, y, :, fcols(h)],
+                      send.at[z, y, h], r_recv.at[z, y, h], plane(to))
+
+    def pass_copy(zt, yt, h, to, send):
+        ref = rows.at[zt, yt, :, fcols(h)]
+        return remote(ref, ref, send.at[zt, yt, h], r_recv.at[zt, yt, h], plane(to))
+
+    def rows_here(zt, yt, h):
+        ref = rows.at[zt, yt, :, fcols(h)]
+        remote(ref, ref, ry_send.at[h], r_recv.at[zt, yt, h], mate).wait_recv()
+
+    def xf_copy(zt, yt, h):
+        return remote(give.at[zt, strip(yt), fcols(h)], slots.at[zt, spot(x, yt), fcols(h)],
+                      xf_send.at[zt, yt, h], xf_recv.at[zt, yt, h], beside)
+
+    def yf_copy(zt, xx, h):
+        ref = slots.at[zt, spot(xx, y), fcols(h)]
+        return remote(ref, ref, yf_send.at[zt, xx, h], yf_recv.at[zt, xx, h], across)
+
+    def mf_copy(zt, h):
+        ref = slots.at[zt, half(c), fcols(h)]
+        return remote(ref, ref, mf_send.at[zt, h], mf_recv.at[zt, h], mate)
+
+    def mb_copy(zt, h):
+        return remote(parts.at[zt, half(1 - c), bcols(h)], mate_in.at[zt, :, bcols(h)],
+                      mb_send.at[zt, h], mb_recv.at[zt, h], mate)
+
+    def yb_copy(zt, xx, h):
+        return remote(parts.at[zt, spot(xx, 1 - y), bcols(h)], y_in.at[zt, strip(xx), bcols(h)],
+                      yb_send.at[zt, xx, h], yb_recv.at[zt, xx, h], across)
+
+    def xb_copy(zt, near, h):
+        if near:
+            return remote(parts.at[zt, both(1 - x), bcols(h)], x_in.at[zt, :, bcols(h)],
+                          xb_send.at[zt, h], xb_recv.at[zt, h], beside)
+        return remote(parts.at[zt, spot(1 - x, y), bcols(h)], x_in.at[zt, strip(y), bcols(h)],
+                      xb_send.at[zt, h], xb_recv.at[zt, h], beside)
+
+    def line_copy(zt, h, to):
+        return remote(sums.at[zt, y, :, bcols(h)], line_in.at[zt, :, bcols(h)],
+                      zf_send.at[zt, h], zf_recv.at[zt, h], plane(to))
+
+    def home_copy(zt, yt, side, h):
+        return remote(sums.at[zt, yt, :, bcols(h)], home_in.at[side, yt, :, bcols(h)],
+                      zh_send.at[side, yt, h], zh_recv.at[side, yt, h], plane(zt))
+
+    def home_here(yt, side, h):
+        ref = home_in.at[side, yt, :, bcols(h)]
+        remote(ref, ref, zh_send.at[side, yt, h], zh_recv.at[side, yt, h], mate).wait_recv()
+
+    def last_copy(h):
+        return remote(sums.at[z, 1 - y, :, bcols(h)], last_in.at[:, bcols(h)],
+                      yl_send.at[h], yl_recv.at[h], across)
 
     loads = [
         pltpu.make_async_copy(wg_hbm.at[0], wg, w_sem.at[0]),
         pltpu.make_async_copy(wu_hbm.at[0], wu, w_sem.at[1]),
         pltpu.make_async_copy(wd_hbm.at[0], wd, w_sem.at[2]),
     ]
-    own = pltpu.make_async_copy(outgoing.at[me], rows.at[me, spot(core, y)], own_sem)
-    own.start()
 
     barrier = pltpu.get_barrier_semaphore()
-
-    @pl.loop(1, n)
-    def _(j):
-        pl.semaphore_signal(barrier, inc=1, device_id=(xor_of(me, j, n), tp),
-                               device_id_type=pl.DeviceIdType.MESH)
-
-    for peer in (mate, across):
-        pl.semaphore_signal(barrier, inc=1, device_id=(me, peer),
-                               device_id_type=pl.DeviceIdType.MESH)
-    pl.semaphore_wait(barrier, n + 1)
-
-    @pl.loop(1, n)
-    def _(j):
-        sp_copy(j).start()
+    for peer in (mate, beside):
+        pl.semaphore_signal(barrier, inc=1, device_id=peer,
+                            device_id_type=pl.DeviceIdType.MESH)
+
+    @pl.loop(1, 8)
+    def _(q):
+        zq, yq = (z + q // 2) % 4, (y + q) % 2
+        pl.semaphore_signal(barrier, inc=1, device_id=(zq * 2 + x, yq * 2 + c),
+                            device_id_type=pl.DeviceIdType.MESH)
+
+    pl.semaphore_wait(barrier, 9)
+
+    @pl.loop(1, 8)
+    def _(q):
+        meta_copy(q).start()
+
+    @pl.loop(0, front)
+    def _(h):
+        dup_copy(h).start()
+        own_copy(h, z1, ra_send).start()
+
+        @pl.when(mid)
+        def _():
+            own_copy(h, z2, rb_send).start()
 
     for load in loads:
         load.start()
-
-    def compute(s):
-        x = rows[s]
-        gate = jnp.dot(x, wg[...], preferred_element_type=jnp.float32)
-        upper = jnp.dot(x, wu[...], preferred_element_type=jnp.float32)
-        hidden = (gate * (1.0 / (1.0 + jnp.exp(-gate))) * upper).astype(jnp.bfloat16)
-        width = wd.shape[1]
-        tile = min(1024, width)
-
-        @pl.loop(0, width // tile)
-        def _(k):
-            cols = pl.ds(pl.multiple_of(k * tile, tile), tile)
-            parts[s, :, cols] = jnp.dot(
-                hidden, wd[:, cols], preferred_element_type=jnp.float32
-            ).astype(jnp.bfloat16)
-
-    @pl.loop(0, n + 3)
-    def _(j):
-        @pl.when(j == 0)
-        def _():
-            own.wait()
-
-        @pl.when((j >= 1) & (j < n))
-        def _():
-            sp_copy(j).wait_recv()
-
-        @pl.when(j < n)
-        def _():
-            fy_copy(j).start()
-            fa_copy(j).start()
-
-        @pl.when((j >= 2) & (j < n + 2))
-        def _():
-            k = j - 2
-            s = chunk(k)
-            pp_copy(k).wait_recv()
-            there = spot(core, 1 - y)
-            far = pl.ds(pl.multiple_of((1 - y) * C, C), C)
-            parts[s, there] = (
-                parts[s, there].astype(jnp.float32) + pair_in[s, far].astype(jnp.float32)
-            ).astype(jnp.bfloat16)
-            ry_copy(k).start()
-
-        @pl.when(j >= 3)
-        def _():
-            k = j - 3
-            s = chunk(k)
-            ry_copy(k).wait_recv()
-            here = spot(core, y)
-            near = pl.ds(pl.multiple_of(y * C, C), C)
+    meta[z, y] = meta_in[...]
+    rows[z, y] = rows_in[...]
+
+    def picks_of(zt, yt):
+        places = meta[zt, yt, tokens:tokens + experts, :]
+        level = lax.broadcasted_iota(jnp.int32, places.shape, 0)
+        slot = lax.broadcasted_iota(jnp.int32, (C, tokens), 0).astype(f32)
+
+        def one(expert):
+            place = jnp.sum(jnp.where(level == expert, places, 0.0), axis=0, keepdims=True)
+            return jnp.where(place[:, :tokens] == slot, 1.0, 0.0)
+
+        return jnp.concatenate([one(me), one(peer_expert)], axis=0).astype(bf16)
+
+    def gather(picks, zt, yt, h):
+        found = jnp.dot(picks, rows[zt, yt, :, fcols(h)], preferred_element_type=f32)
+        found = found.astype(bf16)
+        slots[zt, spot(x, yt), fcols(h)] = found[:C]
+        give[zt, strip(yt), fcols(h)] = found[C:]
+        xf_copy(zt, yt, h).start()
+
+    def arrive(zt, yt, far, onward):
+        meta_here(zt, yt)
+        picks = picks_of(zt, yt)
+
+        @pl.loop(0, front)
+        def _(h):
+            rows_here(zt, yt, h)
+            onward(h)
+            gather(picks, zt, yt, h)
+            if far:
+                yf_copy(zt, x, h).start()
+
+    def nothing(h):
+        pass
+
+    def complete(zt, far):
+        @pl.loop(0, front)
+        def _(h):
+            xf_copy(zt, y, h).wait_recv()
+            if far:
+                yf_copy(zt, 1 - x, h).start()
+            else:
+                xf_copy(zt, 1 - y, h).wait_recv()
+                mf_copy(zt, h).start()
+
+        if far:
+            @pl.loop(0, front)
+            def _(h):
+                yf_copy(zt, x, h).wait_recv()
+                yf_copy(zt, 1 - x, h).wait_recv()
+                mf_copy(zt, h).start()
+
+    def compute(zt):
+        @pl.loop(0, front)
+        def _(h):
+            mf_copy(zt, h).wait_recv()
+
+        v = slots[zt]
+        gate = jnp.dot(v, wg[...], preferred_element_type=f32)
+        upper = jnp.dot(v, wu[...], preferred_element_type=f32)
+        hidden = (gate * (1.0 / (1.0 + jnp.exp(-gate))) * upper).astype(bf16)
+
+        @pl.loop(0, back)
+        def _(h):
+            parts[zt, :, bcols(h)] = jnp.dot(
+                hidden, wd[:, bcols(h)], preferred_element_type=f32
+            ).astype(bf16)
+            mb_copy(zt, h).start()
+
+    def pair_sum(zt, far):
+        @pl.loop(0, back)
+        def _(h):
+            mb_copy(zt, h).wait_recv()
             total = (
-                parts[s, here].astype(jnp.float32)
-                + pair_in[s, near].astype(jnp.float32)
-                + y_in[s].astype(jnp.float32)
-            ).astype(jnp.bfloat16)
-
-            @pl.when(k == 0)
+                parts[zt, half(c), bcols(h)].astype(f32) + mate_in[zt, :, bcols(h)].astype(f32)
+            )
+            parts[zt, half(c), bcols(h)] = total.astype(bf16)
+            if far:
+                yb_copy(zt, 0, h).start()
+                yb_copy(zt, 1, h).start()
+            else:
+                xb_copy(zt, True, h).start()
+
+    def far_sum(zt):
+        @pl.loop(0, back)
+        def _(h):
+            for xx in (0, 1):
+                yb_copy(zt, xx, h).wait_recv()
+                total = (
+                    parts[zt, spot(xx, y), bcols(h)].astype(f32)
+                    + y_in[zt, strip(xx), bcols(h)].astype(f32)
+                )
+                parts[zt, spot(xx, y), bcols(h)] = total.astype(bf16)
+            xb_copy(zt, False, h).start()
+
+    def weights_of(zt, yt):
+        info = meta[zt, yt, :tokens, :]
+        lane = lax.broadcasted_iota(jnp.int32, info.shape, 1)
+        slot = lax.broadcasted_iota(jnp.int32, (tokens, C), 1).astype(f32)
+
+        def one(expert):
+            place = jnp.sum(jnp.where(lane == expert, info, 0.0), axis=1, keepdims=True)
+            weight = jnp.sum(
+                jnp.where(lane == experts + expert, info, 0.0), axis=1, keepdims=True
+            )
+            spread = jnp.where(place == slot, weight, 0.0)
+            head = spread.astype(bf16)
+            return head, (spread - head.astype(f32)).astype(bf16)
+
+        mine, theirs = one(me), one(peer_expert)
+        return jnp.concatenate([mine[0], theirs[0], mine[1], theirs[1]], axis=1)
+
+    def blend(spread, zt, yt, h):
+        mine = parts[zt, spot(x, yt), bcols(h)]
+        theirs = x_in[zt, strip(yt), bcols(h)]
+        pair = jnp.concatenate([mine, theirs, mine, theirs], axis=0)
+        return jnp.dot(spread, pair, preferred_element_type=f32)
+
+    def near_back(zt, side):
+        here = weights_of(zt, y)
+        there = weights_of(zt, 1 - y)
+
+        @pl.loop(0, back)
+        def _(h):
+            xb_copy(zt, True, h).wait_recv()
+            sums[zt, 1 - y, :, bcols(h)] = blend(there, zt, 1 - y, h).astype(bf16)
+            home_copy(zt, 1 - y, side, h).start()
+            total = blend(here, zt, y, h)
+
+            @pl.when(mid)
             def _():
-                out[me] = total
-
-            @pl.when(k > 0)
+                line_copy(zt, h, z1).wait_recv()
+                sums[zt, y, :, bcols(h)] = (
+                    total + line_in[zt, :, bcols(h)].astype(f32)
+                ).astype(bf16)
+
+            @pl.when(end)
             def _():
-                parts[s, here] = total
-                rs_copy(k).start()
-
-        @pl.when((j >= 1) & (j < n + 1))
-        def _():
-            k = j - 1
-            fy_copy(k).wait_recv()
-            fb_copy(k).start()
-
-            @pl.when(k == 0)
+                sums[zt, y, :, bcols(h)] = total.astype(bf16)
+
+            home_copy(zt, y, side, h).start()
+
+    def far_back(zt):
+        here = weights_of(zt, y)
+
+        @pl.loop(0, back)
+        def _(h):
+            xb_copy(zt, False, h).wait_recv()
+            total = blend(here, zt, y, h)
+
+            @pl.when(mid)
             def _():
-                for load in loads:
-                    load.wait()
-
-            fa_copy(k).wait_recv()
-            fb_copy(k).wait_recv()
-            compute(chunk(k))
-            pp_copy(k).start()
-
-    @pl.loop(0, n)
-    def _(j):
-        fy_copy(j).wait_send()
-        fa_copy(j).wait_send()
-        fb_copy(j).wait_send()
-        pp_copy(j).wait_send()
-        ry_copy(j).wait_send()
-
-        @pl.when(j > 0)
-        def _():
-            sp_copy(j).wait_send()
-            rs_copy(j).wait_send()
-            rs_copy(j).wait_recv()
-
-
-def moe_exchange(outgoing, w_gate, w_up, w_down, slices):
-    n, capacity, width = outgoing.shape
+                line_copy(zt, h, z1).wait_recv()
+                sums[zt, y, :, bcols(h)] = (
+                    total + line_in[zt, :, bcols(h)].astype(f32)
+                ).astype(bf16)
+                line_copy(zt, h, z2).start()
+
+            @pl.when(end)
+            def _():
+                sums[zt, y, :, bcols(h)] = total.astype(bf16)
+                line_copy(zt, h, z1).start()
+
+    def own_back():
+        here = weights_of(z, y)
+        there = weights_of(z, 1 - y)
+
+        @pl.loop(0, back)
+        def _(h):
+            xb_copy(z, True, h).wait_recv()
+            sums[z, 1 - y, :, bcols(h)] = blend(there, z, 1 - y, h).astype(bf16)
+            out[:, bcols(h)] = blend(here, z, y, h)
+
+    own_picks = picks_of(z, y)
+
+    @pl.loop(0, front)
+    def _(h):
+        gather(own_picks, z, y, h)
+
+    def dup_on(h):
+        pass_copy(z, 1 - y, h, z1, ra_send).start()
+
+        @pl.when(mid)
+        def _():
+            pass_copy(z, 1 - y, h, z2, rb_send).start()
+
+    arrive(z, 1 - y, False, dup_on)
+
+    def first_on(h):
+        @pl.when(mid)
+        def _():
+            pass_copy(z1, y, h, z2, rb_send).start()
+
+    arrive(z1, y, False, first_on)
+
+    @pl.when(mid)
+    def _():
+        arrive(z2, y, False, lambda h: pass_copy(z2, y, h, z1, ra_send).start())
+
+    complete(z, False)
+    for load in loads:
+        load.wait()
+    compute(z)
+    arrive(z1, 1 - y, False, nothing)
+
+    @pl.when(mid)
+    def _():
+        arrive(z2, 1 - y, False, nothing)
+
+    pair_sum(z, False)
+    complete(z1, False)
+    compute(z1)
+    pair_sum(z1, False)
+
+    @pl.when(end)
+    def _():
+        arrive(z2, y, True, nothing)
+
+    own_back()
+
+    @pl.when(end)
+    def _():
+        near_back(z1, 0)
+        complete(z2, True)
+
+    @pl.when(mid)
+    def _():
+        complete(z2, False)
+
+    compute(z2)
+
+    @pl.when(end)
+    def _():
+        pair_sum(z2, True)
+
+    @pl.when(mid)
+    def _():
+        pair_sum(z2, False)
+
+    def third_on(h):
+        @pl.when(mid)
+        def _():
+            pass_copy(z3, y, h, z1, ra_send).start()
+
+    arrive(z3, y, True, third_on)
+
+    @pl.when(end)
+    def _():
+        far_sum(z2)
+
+    complete(z3, True)
+    compute(z3)
+    pair_sum(z3, True)
+
+    @pl.when(end)
+    def _():
+        far_back(z2)
+
+    far_sum(z3)
+
+    @pl.when(mid)
+    def _():
+        near_back(z2, 1)
+
+    far_back(z3)
+
+    @pl.when(mid)
+    def _():
+        near_back(z1, 0)
+
+    @pl.loop(0, back)
+    def _(h):
+        home_here(1 - y, 0, h)
+        total = (
+            sums[z, 1 - y, :, bcols(h)].astype(f32) + home_in[0, 1 - y, :, bcols(h)].astype(f32)
+        )
+
+        @pl.when(mid)
+        def _():
+            home_here(1 - y, 1, h)
+            sums[z, 1 - y, :, bcols(h)] = (
+                total + home_in[1, 1 - y, :, bcols(h)].astype(f32)
+            ).astype(bf16)
+
+        @pl.when(end)
+        def _():
+            sums[z, 1 - y, :, bcols(h)] = total.astype(bf16)
+
+        last_copy(h).start()
+
+    @pl.loop(0, back)
+    def _(h):
+        home_here(y, 0, h)
+        total = out[:, bcols(h)] + home_in[0, y, :, bcols(h)].astype(f32)
+
+        @pl.when(mid)
+        def _():
+            home_here(y, 1, h)
+            out[:, bcols(h)] = total + home_in[1, y, :, bcols(h)].astype(f32)
+
+        @pl.when(end)
+        def _():
+            out[:, bcols(h)] = total
+
+        last_copy(h).wait_recv()
+        out[:, bcols(h)] += last_in[:, bcols(h)].astype(f32)
+
+    meta_here(z3, 1 - y)
+
+    @pl.when(end)
+    def _():
+        meta_here(z2, 1 - y)
+
+    @pl.loop(1, 8)
+    def _(q):
+        meta_copy(q).wait_send()
+
+    @pl.loop(0, front)
+    def _(h):
+        dup_copy(h).wait_send()
+        own_copy(h, z1, ra_send).wait_send()
+        pass_copy(z, 1 - y, h, z1, ra_send).wait_send()
+        for zt in (z, z1):
+            for yt in (0, 1):
+                xf_copy(zt, yt, h).wait_send()
+        xf_copy(z2, y, h).wait_send()
+        xf_copy(z3, y, h).wait_send()
+        for zt in (z, z1, z2, z3):
+            mf_copy(zt, h).wait_send()
+        yf_copy(z3, 0, h).wait_send()
+        yf_copy(z3, 1, h).wait_send()
+
+        @pl.when(mid)
+        def _():
+            own_copy(h, z2, rb_send).wait_send()
+            pass_copy(z, 1 - y, h, z2, rb_send).wait_send()
+            pass_copy(z1, y, h, z2, rb_send).wait_send()
+            pass_copy(z2, y, h, z1, ra_send).wait_send()
+            pass_copy(z3, y, h, z1, ra_send).wait_send()
+            xf_copy(z2, 1 - y, h).wait_send()
+
+        @pl.when(end)
+        def _():
+            yf_copy(z2, 0, h).wait_send()
+            yf_copy(z2, 1, h).wait_send()
+
+    @pl.loop(0, back)
+    def _(h):
+        for zt in (z, z1, z2, z3):
+            mb_copy(zt, h).wait_send()
+        xb_copy(z, True, h).wait_send()
+        xb_copy(z1, True, h).wait_send()
+        xb_copy(z3, False, h).wait_send()
+        yb_copy(z3, 0, h).wait_send()
+        yb_copy(z3, 1, h).wait_send()
+        line_copy(z3, h, z1).wait_send()
+        home_copy(z1, 0, 0, h).wait_send()
+        home_copy(z1, 1, 0, h).wait_send()
+        last_copy(h).wait_send()
+
+        @pl.when(mid)
+        def _():
+            xb_copy(z2, True, h).wait_send()
+            home_copy(z2, 0, 1, h).wait_send()
+            home_copy(z2, 1, 1, h).wait_send()
+
+        @pl.when(end)
+        def _():
+            xb_copy(z2, False, h).wait_send()
+            yb_copy(z2, 0, h).wait_send()
+            yb_copy(z2, 1, h).wait_send()
+            line_copy(z2, h, z1).wait_send()
+
+
+FRONT, BACK = 2, 4
+
+
+def moe_exchange(normed, meta, w_gate, w_up, w_down, capacity, experts):
+    tokens, width = normed.shape
     units = w_gate.shape[2]
     bf16 = jnp.bfloat16
     dma = pltpu.SemaphoreType.DMA
+    C = capacity
+    vmem = pltpu.VMEM
+    pair = [dma((4, 2, FRONT))] * 2
+    back2 = [dma((4, 2, BACK))] * 2
+    back1 = [dma((4, BACK))] * 2
     return pl.pallas_call(
-        functools.partial(moe_kernel, n, slices, capacity),
-        out_shape=jax.ShapeDtypeStruct(outgoing.shape, bf16),
-        in_specs=[pl.BlockSpec(memory_space=pltpu.VMEM)]
+        functools.partial(moe_kernel, FRONT, BACK, capacity, experts),
+        out_shape=jax.ShapeDtypeStruct((tokens, width), jnp.float32),
+        in_specs=[pl.BlockSpec(memory_space=pltpu.VMEM)] * 2
         + [pl.BlockSpec(memory_space=pl.ANY)] * 3,
         out_specs=pl.BlockSpec(memory_space=pltpu.VMEM),
         scratch_shapes=[
-            pltpu.VMEM((width, units), bf16),
-            pltpu.VMEM((width, units), bf16),
-            pltpu.VMEM((units, width), bf16),
-            pltpu.VMEM((n, slices * capacity, width), bf16),
-            pltpu.VMEM((n, slices * capacity, width), bf16),
-            pltpu.VMEM((n, 2 * capacity, width), bf16),
-            pltpu.VMEM((n, capacity, width), bf16),
-            dma((3,)),
-            dma,
+            vmem((width, units), bf16),
+            vmem((width, units), bf16),
+            vmem((units, width), bf16),
+            vmem((4, 2, tokens, width), bf16),
+            vmem((4, 2) + meta.shape, jnp.float32),
+            vmem((4, 8 * C, width), bf16),
+            vmem((4, 2 * C, width), bf16),
+            vmem((4, 8 * C, width), bf16),
+            vmem((4, 4 * C, width), bf16),
+            vmem((4, 2 * C, width), bf16),
+            vmem((4, 2 * C, width), bf16),
+            vmem((4, 2, tokens, width), bf16),
+            vmem((4, tokens, width), bf16),
+            vmem((2, 2, tokens, width), bf16),
+            vmem((tokens, width), bf16),
+            dma((3,)), dma((8,)), dma((4, 2)), dma((4, 2, FRONT)), dma((FRONT,)),
+            dma((4, 2, FRONT)), dma((4, 2, FRONT)),
         ]
-        + [dma((n,))] * 14,
+        + pair + pair + [dma((4, FRONT))] * 2
+        + back1 + back2 + back1 + back1 + [dma((2, 2, BACK))] * 2 + [dma((BACK,))] * 2,
         compiler_params=pltpu.CompilerParams(
-            collective_id=1, has_side_effects=True, vmem_limit_bytes=52 * 2**20
+            collective_id=1, has_side_effects=True, vmem_limit_bytes=60 * 2**20
         ),
         cost_estimate=pl.CostEstimate(
-            flops=6 * n * slices * capacity * width * units,
+            flops=6 * experts * 4 * C * width * units,
             bytes_accessed=3 * 2 * width * units,
             transcendentals=0,
         ),
         name="moe_exchange",
-    )(outgoing, w_gate, w_up, w_down)
+    )(normed, meta, w_gate, w_up, w_down)
+
+
+def token_table(route_rows, weight_rows, experts):
+    row_count = route_rows.shape[0]
+    f32 = jnp.float32
+    chosen = route_rows[:, :, None] == jnp.arange(experts, dtype=jnp.int32)[None, None, :]
+    hit = jnp.any(chosen, axis=1)
+    order = jnp.arange(row_count)
+    earlier = (order[:, None] > order[None, :]).astype(jnp.bfloat16)
+    place = jnp.dot(earlier, hit.astype(jnp.bfloat16), preferred_element_type=f32)
+    place = jnp.where(hit, place, -1.0)
+    weight = jnp.sum(jnp.where(chosen, weight_rows[:, :, None], 0.0), axis=1)
+    by_token = jnp.pad(
+        jnp.concatenate([place, weight], axis=1), ((0, 0), (0, 128 - 2 * experts))
+    )
+    by_expert = jnp.pad(place.T, ((0, 0), (0, 128 - row_count)), constant_values=-1.0)
+    return jnp.concatenate([by_token, by_expert], axis=0)
 
 
 def sum_kernel(count, part, out, pair_in, total, y_in, pp_send, pp_recv, y_send, y_recv):
@@ -446,11 +819,13 @@
     normed = normalize(mixed, norm_gain)
     route_rows = lax.dynamic_slice_in_dim(routes, first, sub_count, 0)
     weight_rows = lax.dynamic_slice_in_dim(route_weight, first, sub_count, 0)
-    targets = slot_plan(route_rows, 1, capacity, experts)
-    outgoing = fill_slots(normed, targets, experts * capacity).reshape(experts, capacity, width)
-    if slices == 4 and capacity % 16 == 0 and experts & (experts - 1) == 0:
-        returned = moe_exchange(outgoing, w_gate, w_up, w_down, slices)
+    if experts == 8 and slices == 4 and sub_count == 2 * capacity and capacity % 16 == 0:
+        table = token_table(route_rows, weight_rows, experts)
+        moe = moe_exchange(normed, table, w_gate, w_up, w_down, capacity, experts)
     else:
+        targets = slot_plan(route_rows, 1, capacity, experts)
+        outgoing = fill_slots(normed, targets, experts * capacity)
+        outgoing = outgoing.reshape(experts, capacity, width)
         arrived = lax.all_to_all(outgoing, "sp", split_axis=0, concat_axis=0, tiled=True)
         block_rows = lax.all_gather(arrived, "tp", axis=0, tiled=True)
         spread = expert_part(block_rows.reshape(-1, width), w_gate, w_up, w_down).reshape(
@@ -462,7 +837,7 @@
         returned = lax.all_to_all(
             summed.astype(jnp.bfloat16), "sp", split_axis=0, concat_axis=0, tiled=True
         )
-    moe = collect(returned.reshape(-1, width), targets, weight_rows)
+        moe = collect(returned.reshape(-1, width), targets, weight_rows)
     return (mixed + moe).astype(jnp.bfloat16)
 
 

time: 160 us -> 196 us (1.23)
  the two profiles are of different devices: /device:TPU:8 before, /device:TPU:0 now
where the time goes in v1:
time: 196 us
  Pallas kernels  178 us (91%)
  other arithmetic  5.62 us (3%)
  starting transfers between devices  4.86 us (2%)
  local copies, waits for them, and re-layouts  4.48 us (2%)
  matrix products  2.36 us (1%)
    pallas_call x1, Pallas kernels, moe_exchange(): pl.pallas_call(functools.partial(moe_kernel, FRONT, BACK, capacity, exper...  163 us
    pallas_call x1, Pallas kernels, scatter_sum(): pl.pallas_call(functools.partial(sum_kernel, count), out_shape=jax.ShapeD...  15.8 us
    ppermute x1, starting transfers between devices, shifted(): return lax.ppermute(x, axis, pairs)  4.86 us
  transfers between devices with their start and end apart: 1, of which 0 were waited for; matrix products, arithmetic and copies ran while one was open for 1% of the time, Pallas kernels for 0%

profile of v1, /device:TPU:0, one launch (start us, length us, event | category | flops | bytes accessed | tf_op | source)
XLA Modules:
  0.0 195.8 jit_solution(2163511559146324169)
XLA Ops:
  0.0 0.0 copy-start
  0.0 0.8 slice.19
  0.9 4.9 %collective-permute-start = (bf16[16,256]{1,0:T(8,128)(2,1)S(1)}, bf16[16,256]{1,0:T(8,128)(2,1)S(1)}, u32[]{:S(2)}, u32[]{:S(2)}) collective-permute-start(bf16[16,256]{1,0:T(8,128)(2,1)S(1)} %slice.19), channel_id=1, source_target_pairs={{0,4},{4,8},{8,12},{12,16},{16,20},{20,24},{24,28},{1,5},{5,9},{9,... | collective-permute-start | bytes 24584 | tf_op jit(solution)/shard_map/ppermute | solution.py:19
  5.7 0.8 constant_dynamic-slice_fusion.1
  6.5 0.7 constant_dynamic-slice_fusion
  7.2 0.1 convolution_select_fusion
  7.4 0.1 copy.24
  7.5 0.6 select_maximum_fusion.meta_in
  8.1 0.0 collective-permute-done
  8.1 0.9 fusion.12
  9.1 0.0 copy-start.3
  9.1 0.0 copy-start.5
  9.1 0.3 fusion.1
  9.5 0.1 broadcast_add_fusion
  9.6 0.1 copy.22
  9.7 0.0 copy-done
  9.7 0.3 copy-done.3
  10.0 0.0 copy-done.5
  10.0 2.2 %convolution_convert_fusion.part = bf16[256,4096]{1,0:T(8,128)(2,1)} fusion(bf16[256,4096]{1,0:T(8,128)(2,1)S(1)} %copy-done, f32[272,256]{1,0:T(8,128)S(1)} %get-tuple-element.6, f32[384,256]{1,0:T(8,128)S(1)} %bitcast.17, f32[272,256]{1,0:T(8,128)S(1)} %slice.28, s32[]{:T(128)S(6)} %select_n.21, bf16[1,256,256]{2,1,0:T(8,128)(2,1)S(1)} %copy-done.3, ...), kind=kOutput, calls=%fused_computation | convolution fusion | flops 571867136 | bytes 5113860 | tf_op jit(solution)/shard_map/dot_general | solution.py:808
  12.2 0.0 copy-start.1
  12.2 1.6 copy-done.1
  13.8 0.0 copy-start.2
  13.8 0.0 copy-start.4
  13.8 15.8 %scatter_sum.1 = bf16[64,4096]{1,0:T(8,128)(2,1)S(1)} custom-call(bf16[256,4096]{1,0:T(8,128)(2,1)S(1)} %copy-done.1), custom_call_target="tpu_custom_call" | custom-call | bytes 33554432 | tf_op jit(solution)/shard_map/scatter_sum/pallas_call | solution.py:762
  29.6 0.0 copy-done.2
  29.6 0.3 multiply_reduce_fusion
  29.9 0.0 copy-done.4
  29.9 1.0 multiply_convert_fusion.rows_in
  30.9 162.6 %moe_exchange.1 = f32[64,4096]{1,0:T(8,128)} custom-call(bf16[64,4096]{1,0:T(8,128)(2,1)} %multiply_convert_fusion.rows_in, f32[72,128]{1,0:T(8,128)} %select_maximum_fusion.meta_in, bf16[1,4096,256]{2,1,0:T(8,128)(2,1)} %wg_hbm.1, bf16[1,4096,256]{2,1,0:T(8,128)(2,1)} %wu_hbm.1, bf16[1,256,4096]{2,1,0:T(8,128)(2,1)} %wd_hbm.1), custom_call_target="tpu_custom_call" | custom-call | flops 6442450944 | bytes 6291456 | tf_op jit(solution)/shard_map/moe_exchange/pallas_call | solution.py:633
  193.5 2.3 %add_convert_fusion = bf16[64,4096]{1,0:T(8,128)(2,1)} fusion(f32[64,4096]{1,0:T(8,128)} %moe_exchange.1, bf16[64,4096]{1,0:T(8,128)(2,1)S(1)} %scatter_sum.1, bf16[256,4096]{1,0:T(8,128)(2,1)} %param.11, s32[]{:T(128)S(6)} %select_n.20), kind=kLoop, calls=%fused_computation.4 | loop fusion | flops 1310720 | bytes 2621444 | tf_op jit(solution)/shard_map/convert_element_type | solution.py:841
  (9 shorter events, 0.1 us)
Async XLA Ops:
  0.0 9.7 %copy-start = (bf16[256,4096]{1,0:T(8,128)(2,1)S(1)}, bf16[256,4096]{1,0:T(8,128)(2,1)}, u32[]{:S(2)}) copy-start(bf16[256,4096]{1,0:T(8,128)(2,1)} %param.15) | copy-start | bytes 6291460
  0.9 7.3 %collective-permute-start = (bf16[16,256]{1,0:T(8,128)(2,1)S(1)}, bf16[16,256]{1,0:T(8,128)(2,1)S(1)}, u32[]{:S(2)}, u32[]{:S(2)}) collective-permute-start(bf16[16,256]{1,0:T(8,128)(2,1)S(1)} %slice.19), channel_id=1, source_target_pairs={{0,4},{4,8},{8,12},{12,16},{16,20},{20,24},{24,28},{1,5},{5,9},{9,... | collective-permute-start | bytes 24584 | tf_op jit(solution)/shard_map/ppermute | solution.py:19
  9.1 0.9 copy-start.3
  9.1 0.9 copy-start.5
  12.2 1.6 copy-start.1
  13.8 15.8 %copy-start.2 = (bf16[256,4096]{1,0:T(8,128)(2,1)S(1)}, bf16[256,4096]{1,0:T(8,128)(2,1)}, u32[]{:S(2)}) copy-start(bf16[256,4096]{1,0:T(8,128)(2,1)} %param.11) | copy-start | bytes 6291460
  13.8 16.1 %copy-start.4 = (f32[4096]{0:T(1024)S(1)}, f32[4096]{0:T(1024)}, u32[]{:S(2)}) copy-start(f32[4096]{0:T(1024)} %param.16) | copy-start | bytes 49156

commit v2 on v1

--- a/solution.py
+++ b/solution.py
@@ -91,8 +91,8 @@
     front, back, capacity, experts,
     rows_in, meta_in, wg_hbm, wu_hbm, wd_hbm, out,
     wg, wu, wd, rows, meta, slots, give, parts,
-    mate_in, y_in, x_in, sums, line_in, home_in, last_in,
-    w_sem, m_send, m_recv, r_recv, ry_send, ra_send, rb_send,
+    mate_in, y_in, x_in, sums, line_in, home_in, last_in, mixes,
+    w_sem, m_send, m_recv, r_recv, ra_send, rb_send,
     xf_send, xf_recv, yf_send, yf_recv, mf_send, mf_recv,
     mb_send, mb_recv, yb_send, yb_recv, xb_send, xb_recv,
     zf_send, zf_recv, zh_send, zh_recv, yl_send, yl_recv,
@@ -123,9 +123,13 @@
         )
 
     def fcols(h):
+        if h is None:
+            return pl.ds(0, width)
         return pl.ds(pl.multiple_of(h * wf, wf), wf)
 
     def bcols(h):
+        if h is None:
+            return pl.ds(0, width)
         return pl.ds(pl.multiple_of(h * wb, wb), wb)
 
     def spot(xx, yy):
@@ -149,64 +153,59 @@
         remote(meta.at[zt, yt], meta.at[zt, yt], m_send.at[0], m_recv.at[zt, yt],
                mate).wait_recv()
 
-    def dup_copy(h):
-        return remote(rows_in.at[:, fcols(h)], rows.at[z, y, :, fcols(h)],
-                      ry_send.at[h], r_recv.at[z, y, h], across)
+    def at(h):
+        return 0 if h is None else h
 
     def own_copy(h, to, send):
-        return remote(rows_in.at[:, fcols(h)], rows.at[z, y, :, fcols(h)],
-                      send.at[z, y, h], r_recv.at[z, y, h], plane(to))
-
-    def pass_copy(zt, yt, h, to, send):
-        ref = rows.at[zt, yt, :, fcols(h)]
-        return remote(ref, ref, send.at[zt, yt, h], r_recv.at[zt, yt, h], plane(to))
-
-    def rows_here(zt, yt, h):
-        ref = rows.at[zt, yt, :, fcols(h)]
-        remote(ref, ref, ry_send.at[h], r_recv.at[zt, yt, h], mate).wait_recv()
-
-    def xf_copy(zt, yt, h):
-        return remote(give.at[zt, strip(yt), fcols(h)], slots.at[zt, spot(x, yt), fcols(h)],
-                      xf_send.at[zt, yt, h], xf_recv.at[zt, yt, h], beside)
+        return remote(rows_in.at[:, fcols(h)], rows.at[z, :, fcols(h)],
+                      send.at[z], r_recv.at[z, at(h)], plane(to))
+
+    def pass_copy(zt, h, to, send):
+        ref = rows.at[zt, :, fcols(h)]
+        return remote(ref, ref, send.at[zt], r_recv.at[zt, at(h)], plane(to))
+
+    def xf_copy(zt, h):
+        return remote(give.at[zt, :, fcols(h)], slots.at[zt, spot(x, y), fcols(h)],
+                      xf_send.at[zt], xf_recv.at[zt, at(h)], beside)
 
     def yf_copy(zt, xx, h):
         ref = slots.at[zt, spot(xx, y), fcols(h)]
-        return remote(ref, ref, yf_send.at[zt, xx, h], yf_recv.at[zt, xx, h], across)
+        return remote(ref, ref, yf_send.at[zt, xx], yf_recv.at[zt, xx, at(h)], across)
 
     def mf_copy(zt, h):
         ref = slots.at[zt, half(c), fcols(h)]
-        return remote(ref, ref, mf_send.at[zt, h], mf_recv.at[zt, h], mate)
+        return remote(ref, ref, mf_send.at[zt], mf_recv.at[zt, at(h)], mate)
 
     def mb_copy(zt, h):
         return remote(parts.at[zt, half(1 - c), bcols(h)], mate_in.at[zt, :, bcols(h)],
-                      mb_send.at[zt, h], mb_recv.at[zt, h], mate)
+                      mb_send.at[zt], mb_recv.at[zt, at(h)], mate)
 
     def yb_copy(zt, xx, h):
         return remote(parts.at[zt, spot(xx, 1 - y), bcols(h)], y_in.at[zt, strip(xx), bcols(h)],
-                      yb_send.at[zt, xx, h], yb_recv.at[zt, xx, h], across)
+                      yb_send.at[zt, xx], yb_recv.at[zt, xx, at(h)], across)
 
     def xb_copy(zt, near, h):
         if near:
             return remote(parts.at[zt, both(1 - x), bcols(h)], x_in.at[zt, :, bcols(h)],
-                          xb_send.at[zt, h], xb_recv.at[zt, h], beside)
+                          xb_send.at[zt], xb_recv.at[zt, at(h)], beside)
         return remote(parts.at[zt, spot(1 - x, y), bcols(h)], x_in.at[zt, strip(y), bcols(h)],
-                      xb_send.at[zt, h], xb_recv.at[zt, h], beside)
+                      xb_send.at[zt], xb_recv.at[zt, at(h)], beside)
 
     def line_copy(zt, h, to):
         return remote(sums.at[zt, y, :, bcols(h)], line_in.at[zt, :, bcols(h)],
-                      zf_send.at[zt, h], zf_recv.at[zt, h], plane(to))
+                      zf_send.at[zt], zf_recv.at[zt, at(h)], plane(to))
 
     def home_copy(zt, yt, side, h):
         return remote(sums.at[zt, yt, :, bcols(h)], home_in.at[side, yt, :, bcols(h)],
-                      zh_send.at[side, yt, h], zh_recv.at[side, yt, h], plane(zt))
+                      zh_send.at[side, yt], zh_recv.at[side, yt, at(h)], plane(zt))
 
     def home_here(yt, side, h):
         ref = home_in.at[side, yt, :, bcols(h)]
-        remote(ref, ref, zh_send.at[side, yt, h], zh_recv.at[side, yt, h], mate).wait_recv()
+        remote(ref, ref, zh_send.at[side, yt], zh_recv.at[side, yt, at(h)], mate).wait_recv()
 
     def last_copy(h):
         return remote(sums.at[z, 1 - y, :, bcols(h)], last_in.at[:, bcols(h)],
-                      yl_send.at[h], yl_recv.at[h], across)
+                      yl_send, yl_recv.at[at(h)], across)
 
     loads = [
         pltpu.make_async_copy(wg_hbm.at[0], wg, w_sem.at[0]),
@@ -233,7 +232,6 @@
 
     @pl.loop(0, front)
     def _(h):
-        dup_copy(h).start()
         own_copy(h, z1, ra_send).start()
 
         @pl.when(mid)
@@ -243,10 +241,10 @@
     for load in loads:
         load.start()
     meta[z, y] = meta_in[...]
-    rows[z, y] = rows_in[...]
-
-    def picks_of(zt, yt):
-        places = meta[zt, yt, tokens:tokens + experts, :]
+    rows[z] = rows_in[...]
+
+    def picks_of(zt):
+        places = meta[zt, y, :experts, :]
         level = lax.broadcasted_iota(jnp.int32, places.shape, 0)
         slot = lax.broadcasted_iota(jnp.int32, (C, tokens), 0).astype(f32)
 
@@ -256,44 +254,39 @@
 
         return jnp.concatenate([one(me), one(peer_expert)], axis=0).astype(bf16)
 
-    def gather(picks, zt, yt, h):
-        found = jnp.dot(picks, rows[zt, yt, :, fcols(h)], preferred_element_type=f32)
+    def gather(picks, zt, h):
+        found = jnp.dot(picks, rows[zt, :, fcols(h)], preferred_element_type=f32)
         found = found.astype(bf16)
-        slots[zt, spot(x, yt), fcols(h)] = found[:C]
-        give[zt, strip(yt), fcols(h)] = found[C:]
-        xf_copy(zt, yt, h).start()
-
-    def arrive(zt, yt, far, onward):
-        meta_here(zt, yt)
-        picks = picks_of(zt, yt)
+        give[zt, :, fcols(h)] = found[C:]
+        xf_copy(zt, h).start()
+        slots[zt, spot(x, y), fcols(h)] = found[:C]
+        yf_copy(zt, x, h).start()
+
+    def arrive(zt, onward):
+        meta_here(zt, y)
+        picks = picks_of(zt)
 
         @pl.loop(0, front)
         def _(h):
-            rows_here(zt, yt, h)
+            pass_copy(zt, h, z1, ra_send).wait_recv()
             onward(h)
-            gather(picks, zt, yt, h)
-            if far:
-                yf_copy(zt, x, h).start()
+            gather(picks, zt, h)
 
     def nothing(h):
         pass
 
-    def complete(zt, far):
+    def turn(zt):
         @pl.loop(0, front)
         def _(h):
-            xf_copy(zt, y, h).wait_recv()
-            if far:
-                yf_copy(zt, 1 - x, h).start()
-            else:
-                xf_copy(zt, 1 - y, h).wait_recv()
-                mf_copy(zt, h).start()
-
-        if far:
-            @pl.loop(0, front)
-            def _(h):
-                yf_copy(zt, x, h).wait_recv()
-                yf_copy(zt, 1 - x, h).wait_recv()
-                mf_copy(zt, h).start()
+            xf_copy(zt, h).wait_recv()
+            yf_copy(zt, 1 - x, h).start()
+
+    def complete(zt):
+        @pl.loop(0, front)
+        def _(h):
+            yf_copy(zt, x, h).wait_recv()
+            yf_copy(zt, 1 - x, h).wait_recv()
+            mf_copy(zt, h).start()
 
     def compute(zt):
         @pl.loop(0, front)
@@ -312,8 +305,8 @@
             ).astype(bf16)
             mb_copy(zt, h).start()
 
-    def pair_sum(zt, far):
-        @pl.loop(0, back)
+    def pair_sum(zt, far, first=0, stop=back):
+        @pl.loop(first, stop)
         def _(h):
             mb_copy(zt, h).wait_recv()
             total = (
@@ -326,34 +319,37 @@
             else:
                 xb_copy(zt, True, h).start()
 
+    def far_piece(zt, h):
+        for xx in (0, 1):
+            yb_copy(zt, xx, h).wait_recv()
+            total = (
+                parts[zt, spot(xx, y), bcols(h)].astype(f32)
+                + y_in[zt, strip(xx), bcols(h)].astype(f32)
+            )
+            parts[zt, spot(xx, y), bcols(h)] = total.astype(bf16)
+        xb_copy(zt, False, h).start()
+
     def far_sum(zt):
         @pl.loop(0, back)
         def _(h):
-            for xx in (0, 1):
-                yb_copy(zt, xx, h).wait_recv()
-                total = (
-                    parts[zt, spot(xx, y), bcols(h)].astype(f32)
-                    + y_in[zt, strip(xx), bcols(h)].astype(f32)
-                )
-                parts[zt, spot(xx, y), bcols(h)] = total.astype(bf16)
-            xb_copy(zt, False, h).start()
+            far_piece(zt, h)
 
     def weights_of(zt, yt):
-        info = meta[zt, yt, :tokens, :]
-        lane = lax.broadcasted_iota(jnp.int32, info.shape, 1)
-        slot = lax.broadcasted_iota(jnp.int32, (tokens, C), 1).astype(f32)
+        places = meta[zt, yt, :experts, :]
+        shares = meta[zt, yt, experts:, :]
+        level = lax.broadcasted_iota(jnp.int32, places.shape, 0)
+        slot = lax.broadcasted_iota(jnp.int32, (C, places.shape[1]), 0).astype(f32)
 
         def one(expert):
-            place = jnp.sum(jnp.where(lane == expert, info, 0.0), axis=1, keepdims=True)
-            weight = jnp.sum(
-                jnp.where(lane == experts + expert, info, 0.0), axis=1, keepdims=True
-            )
-            spread = jnp.where(place == slot, weight, 0.0)
-            head = spread.astype(bf16)
-            return head, (spread - head.astype(f32)).astype(bf16)
+            place = jnp.sum(jnp.where(level == expert, places, 0.0), axis=0, keepdims=True)
+            share = jnp.sum(jnp.where(level == expert, shares, 0.0), axis=0, keepdims=True)
+            spread = jnp.where(place == slot, share, 0.0)
+            head = spread.astype(bf16).astype(f32)
+            return head, spread - head
 
         mine, theirs = one(me), one(peer_expert)
-        return jnp.concatenate([mine[0], theirs[0], mine[1], theirs[1]], axis=1)
+        both = jnp.concatenate([mine[0], theirs[0], mine[1], theirs[1]], axis=0)
+        return both.T[:tokens].astype(bf16)
 
     def blend(spread, zt, yt, h):
         mine = parts[zt, spot(x, yt), bcols(h)]
@@ -361,15 +357,20 @@
         pair = jnp.concatenate([mine, theirs, mine, theirs], axis=0)
         return jnp.dot(spread, pair, preferred_element_type=f32)
 
-    def near_back(zt, side):
-        here = weights_of(zt, y)
+    def near_other(zt, side, first=0, stop=back):
         there = weights_of(zt, 1 - y)
 
-        @pl.loop(0, back)
+        @pl.loop(first, stop)
         def _(h):
             xb_copy(zt, True, h).wait_recv()
             sums[zt, 1 - y, :, bcols(h)] = blend(there, zt, 1 - y, h).astype(bf16)
             home_copy(zt, 1 - y, side, h).start()
+
+    def near_same(zt, side, first=0, stop=back):
+        here = weights_of(zt, y)
+
+        @pl.loop(first, stop)
+        def _(h):
             total = blend(here, zt, y, h)
 
             @pl.when(mid)
@@ -385,25 +386,49 @@
 
             home_copy(zt, y, side, h).start()
 
-    def far_back(zt):
-        here = weights_of(zt, y)
-
-        @pl.loop(0, back)
-        def _(h):
-            xb_copy(zt, False, h).wait_recv()
-            total = blend(here, zt, y, h)
-
-            @pl.when(mid)
-            def _():
-                line_copy(zt, h, z1).wait_recv()
-                sums[zt, y, :, bcols(h)] = (
-                    total + line_in[zt, :, bcols(h)].astype(f32)
+    def far_back():
+        mixes[0] = weights_of(z3, y)
+        mixes[1] = weights_of(z1, y)
+
+        @pl.loop(0, back + LAG)
+        def _(i):
+            @pl.when(i < back)
+            def _():
+                xb_copy(z3, False, i).wait_recv()
+                total = blend(mixes[0], z3, y, i)
+                line_copy(z3, i, z1).wait_recv()
+                sums[z3, y, :, bcols(i)] = (
+                    total + line_in[z3, :, bcols(i)].astype(f32)
                 ).astype(bf16)
-                line_copy(zt, h, z2).start()
-
-            @pl.when(end)
-            def _():
-                sums[zt, y, :, bcols(h)] = total.astype(bf16)
+                line_copy(z3, i, z2).start()
+
+            @pl.when(i >= LAG)
+            def _():
+                k = i - LAG
+                total = blend(mixes[1], z1, y, k)
+                line_copy(z1, k, z1).wait_recv()
+                sums[z1, y, :, bcols(k)] = (
+                    total + line_in[z1, :, bcols(k)].astype(f32)
+                ).astype(bf16)
+                home_copy(z1, y, 0, k).start()
+
+    def far_chain():
+        mixes[0] = weights_of(z2, y)
+        mixes[1] = weights_of(z3, y)
+
+        @pl.loop(0, 2 * back + LAG)
+        def _(i):
+            @pl.when(i < 2 * back)
+            def _():
+                far_piece(z2 + (z3 - z2) * (i // back), i % back)
+
+            @pl.when(i >= LAG)
+            def _():
+                k = i - LAG
+                which, h = k // back, k % back
+                zt = z2 + (z3 - z2) * which
+                xb_copy(zt, False, h).wait_recv()
+                sums[zt, y, :, bcols(h)] = blend(mixes[which], zt, y, h).astype(bf16)
                 line_copy(zt, h, z1).start()
 
     def own_back():
@@ -416,208 +441,198 @@
             sums[z, 1 - y, :, bcols(h)] = blend(there, z, 1 - y, h).astype(bf16)
             out[:, bcols(h)] = blend(here, z, y, h)
 
-    own_picks = picks_of(z, y)
-
-    @pl.loop(0, front)
-    def _(h):
-        gather(own_picks, z, y, h)
-
-    def dup_on(h):
-        pass_copy(z, 1 - y, h, z1, ra_send).start()
-
-        @pl.when(mid)
-        def _():
-            pass_copy(z, 1 - y, h, z2, rb_send).start()
-
-    arrive(z, 1 - y, False, dup_on)
+    def last_send():
+        @pl.loop(0, back)
+        def _(h):
+            home_here(1 - y, 0, h)
+            total = (
+                sums[z, 1 - y, :, bcols(h)].astype(f32) + home_in[0, 1 - y, :, bcols(h)].astype(f32)
+            )
+
+            @pl.when(mid)
+            def _():
+                home_here(1 - y, 1, h)
+                sums[z, 1 - y, :, bcols(h)] = (
+                    total + home_in[1, 1 - y, :, bcols(h)].astype(f32)
+                ).astype(bf16)
+
+            @pl.when(end)
+            def _():
+                sums[z, 1 - y, :, bcols(h)] = total.astype(bf16)
+
+            last_copy(h).start()
+
+    def finish():
+        @pl.loop(0, back)
+        def _(h):
+            home_here(y, 0, h)
+            total = out[:, bcols(h)] + home_in[0, y, :, bcols(h)].astype(f32)
+
+            @pl.when(mid)
+            def _():
+                home_here(y, 1, h)
+                out[:, bcols(h)] = total + home_in[1, y, :, bcols(h)].astype(f32)
+
+            @pl.when(end)
+            def _():
+                out[:, bcols(h)] = total
+
+            last_copy(h).wait_recv()
+            out[:, bcols(h)] += last_in[:, bcols(h)].astype(f32)
+
+    def scoped(fn, name):
+        def run(*args):
+            with jax.named_scope(name):
+                fn(*args)
+        return run
+
+    arrive = scoped(arrive, "arrive")
+    turn = scoped(turn, "turn")
+    complete = scoped(complete, "complete")
+    compute = scoped(compute, "compute")
+    pair_sum = scoped(pair_sum, "pair_sum")
+    far_sum = scoped(far_sum, "far_sum")
+    near_other = scoped(near_other, "near_other")
+    near_same = scoped(near_same, "near_same")
+    far_back = scoped(far_back, "far_back")
+    own_back = scoped(own_back, "own_back")
+    last_send = scoped(last_send, "last_send")
+    far_chain = scoped(far_chain, "far_chain")
+
+    def onto(zt, to, send):
+        return lambda h: pass_copy(zt, h, to, send).start()
 
     def first_on(h):
         @pl.when(mid)
         def _():
-            pass_copy(z1, y, h, z2, rb_send).start()
-
-    arrive(z1, y, False, first_on)
+            pass_copy(z1, h, z2, rb_send).start()
+
+    meta_picks = picks_of(z)
+
+    @pl.loop(0, front)
+    def _(h):
+        gather(meta_picks, z, h)
+
+    turn(z)
+    arrive(z1, first_on)
 
     @pl.when(mid)
     def _():
-        arrive(z2, y, False, lambda h: pass_copy(z2, y, h, z1, ra_send).start())
-
-    complete(z, False)
+        arrive(z2, onto(z2, z1, ra_send))
+
+    turn(z1)
+
+    @pl.when(mid)
+    def _():
+        turn(z2)
+        arrive(z3, onto(z3, z1, ra_send))
+
+    complete(z)
+    for zt in (z, z1, z2, z3):
+        meta_here(zt, 1 - y)
     for load in loads:
         load.wait()
     compute(z)
-    arrive(z1, 1 - y, False, nothing)
+
+    @pl.when(end)
+    def _():
+        arrive(z2, nothing)
+
+    complete(z1)
+    compute(z1)
+
+    @pl.when(end)
+    def _():
+        turn(z2)
+        pair_sum(z1, False, 0, back // 2)
+        arrive(z3, nothing)
+        pair_sum(z1, False, back // 2, back)
+        near_other(z1, 0, 0, back // 2)
 
     @pl.when(mid)
     def _():
-        arrive(z2, 1 - y, False, nothing)
-
-    pair_sum(z, False)
-    complete(z1, False)
-    compute(z1)
-    pair_sum(z1, False)
+        turn(z3)
+        pair_sum(z1, False)
+
+    complete(z2)
+    compute(z2)
 
     @pl.when(end)
     def _():
-        arrive(z2, y, True, nothing)
-
-    own_back()
-
-    @pl.when(end)
-    def _():
-        near_back(z1, 0)
-        complete(z2, True)
+        turn(z3)
+        pair_sum(z2, True)
+        near_other(z1, 0, back // 2, back)
+        near_same(z1, 0)
+        pair_sum(z, False)
 
     @pl.when(mid)
     def _():
-        complete(z2, False)
-
-    compute(z2)
-
-    @pl.when(end)
-    def _():
-        pair_sum(z2, True)
-
-    @pl.when(mid)
-    def _():
         pair_sum(z2, False)
 
-    def third_on(h):
-        @pl.when(mid)
-        def _():
-            pass_copy(z3, y, h, z1, ra_send).start()
-
-    arrive(z3, y, True, third_on)
-
-    @pl.when(end)
-    def _():
-        far_sum(z2)
-
-    complete(z3, True)
+    complete(z3)
     compute(z3)
     pair_sum(z3, True)
 
     @pl.when(end)
     def _():
-        far_back(z2)
-
-    far_sum(z3)
+        far_chain()
+        own_back()
+        last_send()
 
     @pl.when(mid)
     def _():
-        near_back(z2, 1)
-
-    far_back(z3)
-
-    @pl.when(mid)
-    def _():
-        near_back(z1, 0)
-
-    @pl.loop(0, back)
-    def _(h):
-        home_here(1 - y, 0, h)
-        total = (
-            sums[z, 1 - y, :, bcols(h)].astype(f32) + home_in[0, 1 - y, :, bcols(h)].astype(f32)
-        )
-
-        @pl.when(mid)
-        def _():
-            home_here(1 - y, 1, h)
-            sums[z, 1 - y, :, bcols(h)] = (
-                total + home_in[1, 1 - y, :, bcols(h)].astype(f32)
-            ).astype(bf16)
-
-        @pl.when(end)
-        def _():
-            sums[z, 1 - y, :, bcols(h)] = total.astype(bf16)
-
-        last_copy(h).start()
-
-    @pl.loop(0, back)
-    def _(h):
-        home_here(y, 0, h)
-        total = out[:, bcols(h)] + home_in[0, y, :, bcols(h)].astype(f32)
-
-        @pl.when(mid)
-        def _():
-            home_here(y, 1, h)
-            out[:, bcols(h)] = total + home_in[1, y, :, bcols(h)].astype(f32)
-
-        @pl.when(end)
-        def _():
-            out[:, bcols(h)] = total
-
-        last_copy(h).wait_recv()
-        out[:, bcols(h)] += last_in[:, bcols(h)].astype(f32)
-
-    meta_here(z3, 1 - y)
-
-    @pl.when(end)
-    def _():
-        meta_here(z2, 1 - y)
+        pair_sum(z, False)
+        near_other(z1, 0)
+        near_other(z2, 1)
+        far_sum(z3)
+        own_back()
+        last_send()
+        near_same(z2, 1)
+        far_back()
+
+    with jax.named_scope("finish"):
+        finish()
 
     @pl.loop(1, 8)
     def _(q):
         meta_copy(q).wait_send()
 
-    @pl.loop(0, front)
-    def _(h):
-        dup_copy(h).wait_send()
-        own_copy(h, z1, ra_send).wait_send()
-        pass_copy(z, 1 - y, h, z1, ra_send).wait_send()
-        for zt in (z, z1):
-            for yt in (0, 1):
-                xf_copy(zt, yt, h).wait_send()
-        xf_copy(z2, y, h).wait_send()
-        xf_copy(z3, y, h).wait_send()
-        for zt in (z, z1, z2, z3):
-            mf_copy(zt, h).wait_send()
-        yf_copy(z3, 0, h).wait_send()
-        yf_copy(z3, 1, h).wait_send()
-
-        @pl.when(mid)
-        def _():
-            own_copy(h, z2, rb_send).wait_send()
-            pass_copy(z, 1 - y, h, z2, rb_send).wait_send()
-            pass_copy(z1, y, h, z2, rb_send).wait_send()
-            pass_copy(z2, y, h, z1, ra_send).wait_send()
-            pass_copy(z3, y, h, z1, ra_send).wait_send()
-            xf_copy(z2, 1 - y, h).wait_send()
-
-        @pl.when(end)
-        def _():
-            yf_copy(z2, 0, h).wait_send()
-            yf_copy(z2, 1, h).wait_send()
-
-    @pl.loop(0, back)
-    def _(h):
-        for zt in (z, z1, z2, z3):
-            mb_copy(zt, h).wait_send()
-        xb_copy(z, True, h).wait_send()
-        xb_copy(z1, True, h).wait_send()
-        xb_copy(z3, False, h).wait_send()
-        yb_copy(z3, 0, h).wait_send()
-        yb_copy(z3, 1, h).wait_send()
-        line_copy(z3, h, z1).wait_send()
-        home_copy(z1, 0, 0, h).wait_send()
-        home_copy(z1, 1, 0, h).wait_send()
-        last_copy(h).wait_send()
-
-        @pl.when(mid)
-        def _():
-            xb_copy(z2, True, h).wait_send()
-            home_copy(z2, 0, 1, h).wait_send()
-            home_copy(z2, 1, 1, h).wait_send()
-
-        @pl.when(end)
-        def _():
-            xb_copy(z2, False, h).wait_send()
-            yb_copy(z2, 0, h).wait_send()
-            yb_copy(z2, 1, h).wait_send()
-            line_copy(z2, h, z1).wait_send()
-
-
-FRONT, BACK = 2, 4
+    own_copy(None, z1, ra_send).wait_send()
+    for zt in (z, z1, z2, z3):
+        xf_copy(zt, None).wait_send()
+        yf_copy(zt, 0, None).wait_send()
+        yf_copy(zt, 1, None).wait_send()
+        mf_copy(zt, None).wait_send()
+        mb_copy(zt, None).wait_send()
+    xb_copy(z, True, None).wait_send()
+    xb_copy(z1, True, None).wait_send()
+    xb_copy(z3, False, None).wait_send()
+    yb_copy(z3, 0, None).wait_send()
+    yb_copy(z3, 1, None).wait_send()
+    line_copy(z3, None, z1).wait_send()
+    home_copy(z1, 0, 0, None).wait_send()
+    home_copy(z1, 1, 0, None).wait_send()
+    last_copy(None).wait_send()
+
+    @pl.when(mid)
+    def _():
+        own_copy(None, z2, rb_send).wait_send()
+        pass_copy(z1, None, z2, rb_send).wait_send()
+        pass_copy(z2, None, z1, ra_send).wait_send()
+        pass_copy(z3, None, z1, ra_send).wait_send()
+        xb_copy(z2, True, None).wait_send()
+        home_copy(z2, 0, 1, None).wait_send()
+        home_copy(z2, 1, 1, None).wait_send()
+
+    @pl.when(end)
+    def _():
+        xb_copy(z2, False, None).wait_send()
+        yb_copy(z2, 0, None).wait_send()
+        yb_copy(z2, 1, None).wait_send()
+        line_copy(z2, None, z1).wait_send()
+
+
+FRONT, BACK, LAG = 4, 4, 2
 
 
 def moe_exchange(normed, meta, w_gate, w_up, w_down, capacity, experts):
@@ -627,9 +642,10 @@
     dma = pltpu.SemaphoreType.DMA
     C = capacity
     vmem = pltpu.VMEM
-    pair = [dma((4, 2, FRONT))] * 2
-    back2 = [dma((4, 2, BACK))] * 2
-    back1 = [dma((4, BACK))] * 2
+
+    def lanes(*shape, pieces):
+        return [dma(shape), dma(shape + (pieces,))]
+
     return pl.pallas_call(
         functools.partial(moe_kernel, FRONT, BACK, capacity, experts),
         out_shape=jax.ShapeDtypeStruct((tokens, width), jnp.float32),
@@ -640,10 +656,10 @@
             vmem((width, units), bf16),
             vmem((width, units), bf16),
             vmem((units, width), bf16),
-            vmem((4, 2, tokens, width), bf16),
+            vmem((4, tokens, width), bf16),
             vmem((4, 2) + meta.shape, jnp.float32),
             vmem((4, 8 * C, width), bf16),
-            vmem((4, 2 * C, width), bf16),
+            vmem((4, C, width), bf16),
             vmem((4, 8 * C, width), bf16),
             vmem((4, 4 * C, width), bf16),
             vmem((4, 2 * C, width), bf16),
@@ -652,11 +668,12 @@
             vmem((4, tokens, width), bf16),
             vmem((2, 2, tokens, width), bf16),
             vmem((tokens, width), bf16),
-            dma((3,)), dma((8,)), dma((4, 2)), dma((4, 2, FRONT)), dma((FRONT,)),
-            dma((4, 2, FRONT)), dma((4, 2, FRONT)),
+            vmem((2, tokens, 4 * C), bf16),
+            dma((3,)), dma((8,)), dma((4, 2)), dma((4, FRONT)), dma((4,)), dma((4,)),
         ]
-        + pair + pair + [dma((4, FRONT))] * 2
-        + back1 + back2 + back1 + back1 + [dma((2, 2, BACK))] * 2 + [dma((BACK,))] * 2,
+        + lanes(4, pieces=FRONT) + lanes(4, 2, pieces=FRONT) + lanes(4, pieces=FRONT)
+        + lanes(4, pieces=BACK) + lanes(4, 2, pieces=BACK) + lanes(4, pieces=BACK)
+        + lanes(4, pieces=BACK) + lanes(2, 2, pieces=BACK) + [dma, dma((BACK,))],
         compiler_params=pltpu.CompilerParams(
             collective_id=1, has_side_effects=True, vmem_limit_bytes=60 * 2**20
         ),
@@ -679,11 +696,8 @@
     place = jnp.dot(earlier, hit.astype(jnp.bfloat16), preferred_element_type=f32)
     place = jnp.where(hit, place, -1.0)
     weight = jnp.sum(jnp.where(chosen, weight_rows[:, :, None], 0.0), axis=1)
-    by_token = jnp.pad(
-        jnp.concatenate([place, weight], axis=1), ((0, 0), (0, 128 - 2 * experts))
-    )
-    by_expert = jnp.pad(place.T, ((0, 0), (0, 128 - row_count)), constant_values=-1.0)
-    return jnp.concatenate([by_token, by_expert], axis=0)
+    both = jnp.concatenate([place.T, weight.T], axis=0)
+    return jnp.pad(both, ((0, 0), (0, 128 - row_count)), constant_values=-1.0)
 
 
 def sum_kernel(count, part, out, pair_in, total, y_in, pp_send, pp_recv, y_send, y_recv):

time: 196 us -> 144 us (0.73)
  Pallas kernels: 178 us -> 126 us
    pallas_call x1, Pallas kernels: 163 us -> 111 us  [moe_exchange(): pl.pallas_call(functools.partial(moe_kernel, FRONT, BACK, capacity, exper...]
  transfers between devices with their start and end apart: 1 -> 1, of which waited for: 0 -> 0; matrix products, arithmetic and copies ran while one was open for 1% -> 2% of each run, Pallas kernels for 0% -> 0%
where the time goes in v2:
time: 144 us
  Pallas kernels  126 us (88%)
  other arithmetic  5.59 us (4%)
  starting transfers between devices  4.86 us (3%)
  local copies, waits for them, and re-layouts  4.39 us (3%)
  matrix products  2.36 us (2%)
    pallas_call x1, Pallas kernels, moe_exchange(): pl.pallas_call(functools.partial(moe_kernel, FRONT, BACK, capacity, exper...  111 us
    pallas_call x1, Pallas kernels, scatter_sum(): pl.pallas_call(functools.partial(sum_kernel, count), out_shape=jax.ShapeD...  15.8 us
    ppermute x1, starting transfers between devices, shifted(): return lax.ppermute(x, axis, pairs)  4.86 us
  transfers between devices with their start and end apart: 1, of which 0 were waited for; matrix products, arithmetic and copies ran while one was open for 2% of the time, Pallas kernels for 0%

profile of v2, /device:TPU:0, one launch (start us, length us, event | category | flops | bytes accessed | tf_op | source)
XLA Modules:
  0.0 143.6 jit_solution(9791054966801351425)
XLA Ops:
  0.0 0.0 copy-start
  0.0 0.8 slice.19
  0.9 4.9 %collective-permute-start = (bf16[16,256]{1,0:T(8,128)(2,1)S(1)}, bf16[16,256]{1,0:T(8,128)(2,1)S(1)}, u32[]{:S(2)}, u32[]{:S(2)}) collective-permute-start(bf16[16,256]{1,0:T(8,128)(2,1)S(1)} %slice.19), channel_id=1, source_target_pairs={{0,4},{4,8},{8,12},{12,16},{16,20},{20,24},{24,28},{1,5},{5,9},{9,... | collective-permute-start | bytes 24584 | tf_op jit(solution)/shard_map/ppermute | solution.py:19
  5.7 0.8 constant_dynamic-slice_fusion.1
  6.5 0.7 constant_dynamic-slice_fusion
  7.2 0.1 convolution_select_fusion
  7.4 0.6 select_maximum_fusion.meta_in
  8.0 0.0 collective-permute-done
  8.0 0.9 fusion.12
  8.9 0.0 copy-start.3
  9.0 0.0 copy-start.5
  9.0 0.3 fusion.1
  9.3 0.1 broadcast_add_fusion
  9.4 0.1 copy.20
  9.5 0.0 copy-done
  9.6 0.3 copy-done.3
  9.9 0.0 copy-done.5
  9.9 2.2 %convolution_convert_fusion.part = bf16[256,4096]{1,0:T(8,128)(2,1)} fusion(bf16[256,4096]{1,0:T(8,128)(2,1)S(1)} %copy-done, f32[272,256]{1,0:T(8,128)S(1)} %get-tuple-element.6, f32[384,256]{1,0:T(8,128)S(1)} %bitcast.19, f32[272,256]{1,0:T(8,128)S(1)} %slice.28, s32[]{:T(128)S(6)} %select_n.18, bf16[1,256,256]{2,1,0:T(8,128)(2,1)S(1)} %copy-done.3, ...), kind=kOutput, calls=%fused_computation | convolution fusion | flops 571867136 | bytes 5113860 | tf_op jit(solution)/shard_map/dot_general | solution.py:822
  12.1 0.0 copy-start.1
  12.1 1.6 %copy-done.1 = bf16[256,4096]{1,0:T(8,128)(2,1)S(1)} copy-done((bf16[256,4096]{1,0:T(8,128)(2,1)S(1)}, bf16[256,4096]{1,0:T(8,128)(2,1)}, u32[]{:S(2)}) %copy-start.1) | copy-done | bytes 2097176
  13.7 0.0 copy-start.2
  13.7 0.0 copy-start.4
  13.7 15.8 %scatter_sum.1 = bf16[64,4096]{1,0:T(8,128)(2,1)S(1)} custom-call(bf16[256,4096]{1,0:T(8,128)(2,1)S(1)} %copy-done.1), custom_call_target="tpu_custom_call" | custom-call | bytes 33554432 | tf_op jit(solution)/shard_map/scatter_sum/pallas_call | solution.py:776
  29.5 0.0 copy-done.2
  29.5 0.3 multiply_reduce_fusion
  29.8 0.0 copy-done.4
  29.8 1.0 multiply_convert_fusion.rows_in
  30.8 110.5 %moe_exchange.1 = f32[64,4096]{1,0:T(8,128)} custom-call(bf16[64,4096]{1,0:T(8,128)(2,1)} %multiply_convert_fusion.rows_in, f32[16,128]{1,0:T(8,128)} %select_maximum_fusion.meta_in, bf16[1,4096,256]{2,1,0:T(8,128)(2,1)} %wg_hbm.1, bf16[1,4096,256]{2,1,0:T(8,128)(2,1)} %wu_hbm.1, bf16[1,256,4096]{2,1,0:T(8,128)(2,1)} %wd_hbm.1), custom_call_target="tpu_custom_call" | custom-call | flops 6442450944 | bytes 6291456 | tf_op jit(solution)/shard_map/moe_exchange/pallas_call | solution.py:649
  141.3 2.3 %add_convert_fusion = bf16[64,4096]{1,0:T(8,128)(2,1)} fusion(f32[64,4096]{1,0:T(8,128)} %moe_exchange.1, bf16[64,4096]{1,0:T(8,128)(2,1)S(1)} %scatter_sum.1, bf16[256,4096]{1,0:T(8,128)(2,1)} %param.11, s32[]{:T(128)S(6)} %select_n.17), kind=kLoop, calls=%fused_computation.4 | loop fusion | flops 1310720 | bytes 2621444 | tf_op jit(solution)/shard_map/convert_element_type | solution.py:855
  (8 shorter events, 0.1 us)
Async XLA Ops:
  0.0 9.6 %copy-start = (bf16[256,4096]{1,0:T(8,128)(2,1)S(1)}, bf16[256,4096]{1,0:T(8,128)(2,1)}, u32[]{:S(2)}) copy-start(bf16[256,4096]{1,0:T(8,128)(2,1)} %param.15) | copy-start | bytes 6291460
  0.9 7.1 %collective-permute-start = (bf16[16,256]{1,0:T(8,128)(2,1)S(1)}, bf16[16,256]{1,0:T(8,128)(2,1)S(1)}, u32[]{:S(2)}, u32[]{:S(2)}) collective-permute-start(bf16[16,256]{1,0:T(8,128)(2,1)S(1)} %slice.19), channel_id=1, source_target_pairs={{0,4},{4,8},{8,12},{12,16},{16,20},{20,24},{24,28},{1,5},{5,9},{9,... | collective-permute-start | bytes 24584 | tf_op jit(solution)/shard_map/ppermute | solution.py:19
  8.9 0.9 copy-start.3
  9.0 0.9 copy-start.5
  12.1 1.6 %copy-start.1 = (bf16[256,4096]{1,0:T(8,128)(2,1)S(1)}, bf16[256,4096]{1,0:T(8,128)(2,1)}, u32[]{:S(2)}) copy-start(bf16[256,4096]{1,0:T(8,128)(2,1)} %convolution_convert_fusion.part) | copy-start | bytes 6291460
  13.7 15.8 %copy-start.2 = (bf16[256,4096]{1,0:T(8,128)(2,1)S(1)}, bf16[256,4096]{1,0:T(8,128)(2,1)}, u32[]{:S(2)}) copy-start(bf16[256,4096]{1,0:T(8,128)(2,1)} %param.11) | copy-start | bytes 6291460
  13.7 16.1 %copy-start.4 = (f32[4096]{0:T(1024)S(1)}, f32[4096]{0:T(1024)}, u32[]{:S(2)}) copy-start(f32[4096]{0:T(1024)} %param.16) | copy-start | bytes 49156

commit v3 on v2

--- a/solution.py
+++ b/solution.py
@@ -89,10 +89,14 @@
 
 def moe_kernel(
     front, back, capacity, experts,
-    rows_in, meta_in, wg_hbm, wu_hbm, wd_hbm, out,
+    resid, pool_in, pool_mix, pool_gain, out_proj, norm_gain,
+    wg_hbm, wu_hbm, wd_hbm, routes, shares_in, out,
+    pool, mix, gain, proj, scales, named, shares, stay, halo, pooled, part,
+    pair_in, far_out, far_in, mixed, meta_in,
     wg, wu, wd, rows, meta, slots, give, parts,
     mate_in, y_in, x_in, sums, line_in, home_in, last_in, mixes,
-    w_sem, m_send, m_recv, r_recv, ra_send, rb_send,
+    w_sem, h_send, h_recv, pp_send, pp_recv, fy_send, fy_recv,
+    m_send, m_recv, r_recv, ra_send, rb_send,
     xf_send, xf_recv, yf_send, yf_recv, mf_send, mf_recv,
     mb_send, mb_recv, yb_send, yb_recv, xb_send, xb_recv,
     zf_send, zf_recv, zh_send, zh_recv, yl_send, yl_recv,
@@ -102,7 +106,12 @@
     z, x = me // 2, me % 2
     y, c = tp // 2, tp % 2
     C = capacity
-    tokens, width = rows_in.shape
+    tokens, width = out.shape
+    count = lax.axis_size("sp")
+    row_count = pool.shape[0]
+    reach = halo.shape[0]
+    first = pl.multiple_of(tp * tokens, tokens)
+    pieces = tokens // 16
     wf, wb = width // front, width // back
     z1, z2, z3 = line_plan(z)
     mid = ((z + 1) // 2) % 2 == 1
@@ -156,12 +165,34 @@
     def at(h):
         return 0 if h is None else h
 
-    def own_copy(h, to, send):
-        return remote(rows_in.at[:, fcols(h)], rows.at[z, :, fcols(h)],
-                      send.at[z], r_recv.at[z, at(h)], plane(to))
+    def piece(k):
+        if k is None:
+            return pl.ds(0, tokens)
+        return pl.ds(pl.multiple_of(k * 16, 16), 16)
+
+    def block(yy, cc):
+        return pl.multiple_of((yy * 2 + cc) * tokens, tokens)
+
+    def block_piece(yy, cc, k):
+        return pl.ds(pl.multiple_of(block(yy, cc) + k * 16, 16), 16)
+
+    def halo_copy():
+        return remote(pool.at[pl.ds(row_count - reach, reach)], halo, h_send, h_recv,
+                      (me + 1, tp))
+
+    def pair_copy(yy, place, k):
+        if k is None:
+            return remote(part.at[pl.ds(block(yy, 1 - c), tokens)], pair_in.at[place],
+                          pp_send.at[place], pp_recv.at[place, 0], mate)
+        return remote(part.at[block_piece(yy, 1 - c, k)], pair_in.at[place, piece(k)],
+                      pp_send.at[place], pp_recv.at[place, k], mate)
+
+    def far_copy(k):
+        return remote(far_out.at[piece(k)], far_in.at[piece(k)],
+                      fy_send, fy_recv.at[at(k)], across)
 
     def pass_copy(zt, h, to, send):
-        ref = rows.at[zt, :, fcols(h)]
+        ref = rows.at[zt, piece(h)]
         return remote(ref, ref, send.at[zt], r_recv.at[zt, at(h)], plane(to))
 
     def xf_copy(zt, h):
@@ -207,15 +238,32 @@
         return remote(sums.at[z, 1 - y, :, bcols(h)], last_in.at[:, bcols(h)],
                       yl_send, yl_recv.at[at(h)], across)
 
+    small = [
+        pltpu.make_async_copy(pool_in, pool, w_sem.at[3]),
+        pltpu.make_async_copy(routes, named, w_sem.at[4]),
+        pltpu.make_async_copy(shares_in, shares, w_sem.at[5]),
+        pltpu.make_async_copy(pool_mix.at[0], mix, w_sem.at[6]),
+        pltpu.make_async_copy(pool_gain, gain, w_sem.at[7]),
+        pltpu.make_async_copy(out_proj, proj, w_sem.at[8]),
+        pltpu.make_async_copy(resid.at[pl.ds(first, tokens)], stay, w_sem.at[9]),
+        pltpu.make_async_copy(norm_gain, scales, w_sem.at[10]),
+    ]
     loads = [
         pltpu.make_async_copy(wg_hbm.at[0], wg, w_sem.at[0]),
         pltpu.make_async_copy(wu_hbm.at[0], wu, w_sem.at[1]),
         pltpu.make_async_copy(wd_hbm.at[0], wd, w_sem.at[2]),
     ]
+    for load in small + loads:
+        load.start()
 
     barrier = pltpu.get_barrier_semaphore()
     for peer in (mate, beside):
         pl.semaphore_signal(barrier, inc=1, device_id=peer,
+                            device_id_type=pl.DeviceIdType.MESH)
+
+    @pl.when(me > 0)
+    def _():
+        pl.semaphore_signal(barrier, inc=1, device_id=(me - 1, tp),
                             device_id_type=pl.DeviceIdType.MESH)
 
     @pl.loop(1, 8)
@@ -224,24 +272,110 @@
         pl.semaphore_signal(barrier, inc=1, device_id=(zq * 2 + x, yq * 2 + c),
                             device_id_type=pl.DeviceIdType.MESH)
 
-    pl.semaphore_wait(barrier, 9)
+    pl.semaphore_wait(barrier, 9 + (2 * count - 2 - me) // count)
+    small[0].wait()
+
+    @pl.when(me < count - 1)
+    def _():
+        halo_copy().start()
+
+    for load in small[1:]:
+        load.wait()
+
+    level = lax.broadcasted_iota(jnp.int32, (experts, row_count), 0)
+    one_is, two_is = named[0:1, :] == level, named[1:2, :] == level
+    hit = jnp.where(one_is | two_is, 1.0, 0.0)
+    share = jnp.where(one_is, shares[0:1, :], 0.0) + jnp.where(two_is, shares[1:2, :], 0.0)
+    head = share.astype(bf16).astype(f32)
+    stack = jnp.concatenate([hit, head, share - head, hit], axis=0).astype(bf16)
+    row = lax.broadcasted_iota(jnp.int32, (row_count, 128), 0)
+    lane = lax.broadcasted_iota(jnp.int32, (row_count, 128), 1)
+    inside = lane < tokens
+    here = jnp.where((row == lane + first) & inside, 1.0, 0.0).astype(bf16)
+    ahead = jnp.where((row >= first) & (row < lane + first) & inside, 1.0, 0.0).astype(bf16)
+    taken = jnp.dot(stack, here, preferred_element_type=f32)
+    before = jnp.dot(stack, ahead, preferred_element_type=f32)
+    table = jnp.concatenate(
+        [
+            jnp.where(taken[:experts] > 0.5, before[:experts], -1.0),
+            taken[experts:2 * experts] + taken[2 * experts:3 * experts],
+        ],
+        axis=0,
+    )
+    meta_in[...] = table
+    meta[z, y] = table
+
+    @pl.when(me == 0)
+    def _():
+        halo[...] = jnp.zeros(halo.shape, bf16)
+
+    @pl.when(me > 0)
+    def _():
+        halo_copy().wait_recv()
+
+    joined = jnp.concatenate([halo[...], pool[...]], axis=0).astype(f32)
+    runs = [joined]
+    for by in (1, 2, 4, 8):
+        runs.append(runs[-1] + pltpu.roll(runs[-1], by, 0))
+    total = jnp.where(
+        tp == 0, runs[1], jnp.where(tp == 1, runs[2], jnp.where(tp == 2, runs[3], runs[4]))
+    )[reach:]
+    span = jnp.where(tp == 0, 2, jnp.where(tp == 1, 4, jnp.where(tp == 2, 8, 16)))
+    place = lax.broadcasted_iota(jnp.int32, (row_count, 1), 0) + me * row_count + 1
+    counted = jnp.minimum(place, span).astype(f32)
+    diff = (total / counted - joined[reach:]).astype(bf16)
+    pooled[...] = (
+        jnp.dot(diff, mix[...], preferred_element_type=f32) * gain[...]
+    ).astype(bf16)
+
+    def project(yy, cc):
+        span = pl.ds(block(yy, cc), tokens)
+
+        @pl.loop(0, front)
+        def _(h):
+            part[span, fcols(h)] = jnp.dot(
+                pooled[span, :], proj[:, fcols(h)], preferred_element_type=f32
+            ).astype(bf16)
+
+    for yy, place in ((1 - y, 0), (y, 1)):
+        project(yy, 1 - c)
+
+        @pl.loop(0, pieces)
+        def _(k):
+            pair_copy(yy, place, k).start()
+
+        project(yy, c)
 
     @pl.loop(1, 8)
     def _(q):
         meta_copy(q).start()
 
-    @pl.loop(0, front)
-    def _(h):
-        own_copy(h, z1, ra_send).start()
+    @pl.loop(0, pieces)
+    def _(k):
+        pair_copy(1 - y, 0, k).wait_recv()
+        far_out[piece(k)] = (
+            part[block_piece(1 - y, c, k)].astype(f32) + pair_in[0, piece(k)].astype(f32)
+        ).astype(bf16)
+        far_copy(k).start()
+
+    @pl.loop(0, pieces)
+    def _(k):
+        pair_copy(y, 1, k).wait_recv()
+        far_copy(k).wait_recv()
+        added = (
+            part[block_piece(y, c, k)].astype(f32)
+            + pair_in[1, piece(k)].astype(f32)
+            + far_in[piece(k)].astype(f32)
+        ).astype(bf16)
+        values = stay[piece(k)].astype(f32) + added.astype(f32)
+        mixed[piece(k)] = values
+        scale = lax.rsqrt(jnp.mean(values * values, axis=1, keepdims=True) + EPS)
+        rows[z, piece(k)] = (values * scale * scales[...]).astype(bf16)
+        pass_copy(z, k, z1, ra_send).start()
 
         @pl.when(mid)
         def _():
-            own_copy(h, z2, rb_send).start()
-
-    for load in loads:
-        load.start()
-    meta[z, y] = meta_in[...]
-    rows[z] = rows_in[...]
+            pass_copy(z, k, z2, rb_send).start()
 
     def picks_of(zt):
         places = meta[zt, y, :experts, :]
@@ -266,10 +400,13 @@
         meta_here(zt, y)
         picks = picks_of(zt)
 
+        @pl.loop(0, pieces)
+        def _(k):
+            pass_copy(zt, k, z1, ra_send).wait_recv()
+            onward(k)
+
         @pl.loop(0, front)
         def _(h):
-            pass_copy(zt, h, z1, ra_send).wait_recv()
-            onward(h)
             gather(picks, zt, h)
 
     def nothing(h):
@@ -439,7 +576,7 @@
         def _(h):
             xb_copy(z, True, h).wait_recv()
             sums[z, 1 - y, :, bcols(h)] = blend(there, z, 1 - y, h).astype(bf16)
-            out[:, bcols(h)] = blend(here, z, y, h)
+            mixed[:, bcols(h)] += blend(here, z, y, h)
 
     def last_send():
         @pl.loop(0, back)
@@ -466,19 +603,21 @@
         @pl.loop(0, back)
         def _(h):
             home_here(y, 0, h)
-            total = out[:, bcols(h)] + home_in[0, y, :, bcols(h)].astype(f32)
+            last_copy(h).wait_recv()
+            total = (
+                mixed[:, bcols(h)]
+                + home_in[0, y, :, bcols(h)].astype(f32)
+                + last_in[:, bcols(h)].astype(f32)
+            )
 
             @pl.when(mid)
             def _():
                 home_here(y, 1, h)
-                out[:, bcols(h)] = total + home_in[1, y, :, bcols(h)].astype(f32)
+                out[:, bcols(h)] = (total + home_in[1, y, :, bcols(h)].astype(f32)).astype(bf16)
 
             @pl.when(end)
             def _():
-                out[:, bcols(h)] = total
-
-            last_copy(h).wait_recv()
-            out[:, bcols(h)] += last_in[:, bcols(h)].astype(f32)
+                out[:, bcols(h)] = total.astype(bf16)
 
     def scoped(fn, name):
         def run(*args):
@@ -597,7 +736,14 @@
     def _(q):
         meta_copy(q).wait_send()
 
-    own_copy(None, z1, ra_send).wait_send()
+    @pl.when(me < count - 1)
+    def _():
+        halo_copy().wait_send()
+
+    pair_copy(1 - y, 0, None).wait_send()
+    pair_copy(y, 1, None).wait_send()
+    far_copy(None).wait_send()
+    pass_copy(z, None, z1, ra_send).wait_send()
     for zt in (z, z1, z2, z3):
         xf_copy(zt, None).wait_send()
         yf_copy(zt, 0, None).wait_send()
@@ -616,7 +762,7 @@
 
     @pl.when(mid)
     def _():
-        own_copy(None, z2, rb_send).wait_send()
+        pass_copy(z, None, z2, rb_send).wait_send()
         pass_copy(z1, None, z2, rb_send).wait_send()
         pass_copy(z2, None, z1, ra_send).wait_send()
         pass_copy(z3, None, z1, ra_send).wait_send()
@@ -635,29 +781,50 @@
 FRONT, BACK, LAG = 4, 4, 2
 
 
-def moe_exchange(normed, meta, w_gate, w_up, w_down, capacity, experts):
-    tokens, width = normed.shape
+def layer_kernel(
+    resid, pool_in, pool_mix, pool_gain, out_proj, norm_gain,
+    w_gate, w_up, w_down, routes, route_weight, capacity, experts, slices,
+):
+    row_count, width = resid.shape
+    tokens = row_count // slices
+    channels = pool_in.shape[1]
     units = w_gate.shape[2]
-    bf16 = jnp.bfloat16
+    bf16, f32 = jnp.bfloat16, jnp.float32
     dma = pltpu.SemaphoreType.DMA
     C = capacity
     vmem = pltpu.VMEM
+    pieces = tokens // 16
 
     def lanes(*shape, pieces):
         return [dma(shape), dma(shape + (pieces,))]
 
     return pl.pallas_call(
         functools.partial(moe_kernel, FRONT, BACK, capacity, experts),
-        out_shape=jax.ShapeDtypeStruct((tokens, width), jnp.float32),
-        in_specs=[pl.BlockSpec(memory_space=pltpu.VMEM)] * 2
-        + [pl.BlockSpec(memory_space=pl.ANY)] * 3,
+        out_shape=jax.ShapeDtypeStruct((tokens, width), bf16),
+        in_specs=[pl.BlockSpec(memory_space=pl.ANY)] * 11,
         out_specs=pl.BlockSpec(memory_space=pltpu.VMEM),
         scratch_shapes=[
+            vmem((row_count, channels), bf16),
+            vmem((channels, channels), bf16),
+            vmem((1, channels), f32),
+            vmem((channels, width), bf16),
+            vmem((1, width), f32),
+            vmem((2, row_count), jnp.int32),
+            vmem((2, row_count), f32),
+            vmem((tokens, width), bf16),
+            vmem((2**GROUPS, channels), bf16),
+            vmem((row_count, channels), bf16),
+            vmem((row_count, width), bf16),
+            vmem((2, tokens, width), bf16),
+            vmem((tokens, width), bf16),
+            vmem((tokens, width), bf16),
+            vmem((tokens, width), f32),
+            vmem((2 * experts, 128), f32),
             vmem((width, units), bf16),
             vmem((width, units), bf16),
             vmem((units, width), bf16),
             vmem((4, tokens, width), bf16),
-            vmem((4, 2) + meta.shape, jnp.float32),
+            vmem((4, 2, 2 * experts, 128), f32),
             vmem((4, 8 * C, width), bf16),
             vmem((4, C, width), bf16),
             vmem((4, 8 * C, width), bf16),
@@ -669,35 +836,25 @@
             vmem((2, 2, tokens, width), bf16),
             vmem((tokens, width), bf16),
             vmem((2, tokens, 4 * C), bf16),
-            dma((3,)), dma((8,)), dma((4, 2)), dma((4, FRONT)), dma((4,)), dma((4,)),
+            dma((11,)), dma, dma, dma((2,)), dma((2, pieces)), dma, dma((pieces,)),
+            dma((8,)), dma((4, 2)), dma((4, pieces)), dma((4,)), dma((4,)),
         ]
         + lanes(4, pieces=FRONT) + lanes(4, 2, pieces=FRONT) + lanes(4, pieces=FRONT)
         + lanes(4, pieces=BACK) + lanes(4, 2, pieces=BACK) + lanes(4, pieces=BACK)
         + lanes(4, pieces=BACK) + lanes(2, 2, pieces=BACK) + [dma, dma((BACK,))],
         compiler_params=pltpu.CompilerParams(
-            collective_id=1, has_side_effects=True, vmem_limit_bytes=60 * 2**20
+            collective_id=1, has_side_effects=True, vmem_limit_bytes=63 * 2**20
         ),
         cost_estimate=pl.CostEstimate(
             flops=6 * experts * 4 * C * width * units,
-            bytes_accessed=3 * 2 * width * units,
+            bytes_accessed=4 * 2 * width * units,
             transcendentals=0,
         ),
         name="moe_exchange",
-    )(normed, meta, w_gate, w_up, w_down)
-
-
-def token_table(route_rows, weight_rows, experts):
-    row_count = route_rows.shape[0]
-    f32 = jnp.float32
-    chosen = route_rows[:, :, None] == jnp.arange(experts, dtype=jnp.int32)[None, None, :]
-    hit = jnp.any(chosen, axis=1)
-    order = jnp.arange(row_count)
-    earlier = (order[:, None] > order[None, :]).astype(jnp.bfloat16)
-    place = jnp.dot(earlier, hit.astype(jnp.bfloat16), preferred_element_type=f32)
-    place = jnp.where(hit, place, -1.0)
-    weight = jnp.sum(jnp.where(chosen, weight_rows[:, :, None], 0.0), axis=1)
-    both = jnp.concatenate([place.T, weight.T], axis=0)
-    return jnp.pad(both, ((0, 0), (0, 128 - row_count)), constant_values=-1.0)
+    )(
+        resid, pool_in, pool_mix, pool_gain[None], out_proj, norm_gain[None],
+        w_gate, w_up, w_down, routes.T, route_weight.T,
+    )
 
 
 def sum_kernel(count, part, out, pair_in, total, y_in, pp_send, pp_recv, y_send, y_recv):
@@ -814,6 +971,12 @@
     slices = lax.axis_size("tp")
     sub_count = token_count // slices
     capacity = max(2, 2 * sub_count * choose // experts)
+    whole = experts == 8 and slices == 4 and choose == 2 and token_count % 16 == 0
+    if whole and sub_count == 2 * capacity and 4 * capacity == 128:
+        return layer_kernel(
+            resid, pool_in, pool_mix, pool_gain, out_proj, norm_gain,
+            w_gate, w_up, w_down, routes, route_weight, capacity, experts, slices,
+        )
     tp_index = lax.axis_index("tp")
     diff = group_diff(pool_in)
     pooled = (jnp.dot(diff, pool_mix[0], preferred_element_type=jnp.float32) * pool_gain).astype(
@@ -833,25 +996,21 @@
     normed = normalize(mixed, norm_gain)
     route_rows = lax.dynamic_slice_in_dim(routes, first, sub_count, 0)
     weight_rows = lax.dynamic_slice_in_dim(route_weight, first, sub_count, 0)
-    if experts == 8 and slices == 4 and sub_count == 2 * capacity and capacity % 16 == 0:
-        table = token_table(route_rows, weight_rows, experts)
-        moe = moe_exchange(normed, table, w_gate, w_up, w_down, capacity, experts)
-    else:
-        targets = slot_plan(route_rows, 1, capacity, experts)
-        outgoing = fill_slots(normed, targets, experts * capacity)
-        outgoing = outgoing.reshape(experts, capacity, width)
-        arrived = lax.all_to_all(outgoing, "sp", split_axis=0, concat_axis=0, tiled=True)
-        block_rows = lax.all_gather(arrived, "tp", axis=0, tiled=True)
-        spread = expert_part(block_rows.reshape(-1, width), w_gate, w_up, w_down).reshape(
-            block_rows.shape
-        )
-        stacked = spread.reshape((slices,) + arrived.shape)
-        received = lax.all_to_all(stacked, "tp", split_axis=0, concat_axis=0, tiled=True)
-        summed = jnp.sum(received.astype(jnp.float32), axis=0)
-        returned = lax.all_to_all(
-            summed.astype(jnp.bfloat16), "sp", split_axis=0, concat_axis=0, tiled=True
-        )
-        moe = collect(returned.reshape(-1, width), targets, weight_rows)
+    targets = slot_plan(route_rows, 1, capacity, experts)
+    outgoing = fill_slots(normed, targets, experts * capacity)
+    outgoing = outgoing.reshape(experts, capacity, width)
+    arrived = lax.all_to_all(outgoing, "sp", split_axis=0, concat_axis=0, tiled=True)
+    block_rows = lax.all_gather(arrived, "tp", axis=0, tiled=True)
+    spread = expert_part(block_rows.reshape(-1, width), w_gate, w_up, w_down).reshape(
+        block_rows.shape
+    )
+    stacked = spread.reshape((slices,) + arrived.shape)
+    received = lax.all_to_all(stacked, "tp", split_axis=0, concat_axis=0, tiled=True)
+    summed = jnp.sum(received.astype(jnp.float32), axis=0)
+    returned = lax.all_to_all(
+        summed.astype(jnp.bfloat16), "sp", split_axis=0, concat_axis=0, tiled=True
+    )
+    moe = collect(returned.reshape(-1, width), targets, weight_rows)
     return (mixed + moe).astype(jnp.bfloat16)
 
 

time: 144 us -> 129 us (0.90)
  other arithmetic: 5.59 us -> 0 us
  starting transfers between devices: 4.86 us -> 0 us
  local copies, waits for them, and re-layouts: 4.39 us -> 1.87 us
  matrix products: 2.36 us -> 0 us
    ppermute x1 -> x0, starting transfers between devices: 4.86 us -> none  [shifted(): return lax.ppermute(x, axis, pairs)]
    convert_element_type x3 -> x0, other arithmetic: 3.33 us -> none  [the longest x1 2.31 us: on_device(): return (mixed + moe).astype(jnp.bfloat16)]
    dot_general x2 -> x0, matrix products: 2.36 us -> none  [the longest x1 2.23 us: on_device(): jnp.dot(pooled, out_proj, preferred_element_type=jnp.float32)]
    dynamic_slice x2 -> x0, local copies, waits for them, and re-layouts: 1.51 us -> none  [the longest x1 0.76 us: on_device(): route_rows = lax.dynamic_slice_in_dim(routes, first, sub_count, 0)]
    pallas_call x2 -> x1, Pallas kernels: 126 us -> 127 us  [layer_kernel(): pl.pallas_call(functools.partial(moe_kernel, FRONT, BACK, capacity, exper...]
  transfers between devices with their start and end apart: 1 -> 0, of which waited for: 0 -> 0; matrix products, arithmetic and copies ran while one was open for 2% -> 0% of each run, Pallas kernels for 0% -> 0%
where the time goes in v3:
time: 129 us
  Pallas kernels  127 us (98%)
  local copies, waits for them, and re-layouts  1.87 us (1%)
    pallas_call x1, Pallas kernels, layer_kernel(): pl.pallas_call(functools.partial(moe_kernel, FRONT, BACK, capacity, exper...  127 us

profile of v3, /device:TPU:0, one launch (start us, length us, event | category | flops | bytes accessed | tf_op | source)
XLA Modules:
  0.0 129.2 jit_solution(15704554713989020032)
XLA Ops:
  0.0 127.3 %moe_exchange.1 = bf16[64,4096]{1,0:T(8,128)(2,1)} custom-call(bf16[256,4096]{1,0:T(8,128)(2,1)} %resid.1, bf16[256,256]{1,0:T(8,128)(2,1)} %pool_in.1, bf16[1,256,256]{2,1,0:T(8,128)(2,1)} %pool_mix.1, f32[1,256]{1,0:T(1,128)} %bitcast.7, bf16[256,4096]{1,0:T(8,128)(2,1)} %out_proj.1, f32[1,4096]{1,0:T(1,128)} %bitcast.4, bf16[1,4096,256]{2,1,0:T(8,128)(2,1)} %wg_hbm.1, ...), custom_call_target="tpu_custom_call" | custom-call | flops 6442450944 | bytes 8388608 | tf_op jit(solution)/shard_map/moe_exchange/pallas_call | solution.py:801
  127.3 1.9 %copy.13 = bf16[64,4096]{1,0:T(8,128)(2,1)} copy(bf16[64,4096]{1,0:T(8,128)(2,1)} %moe_exchange.1) | data formatting | bytes 1048576

commit v4 on v3

--- a/solution.py
+++ b/solution.py
@@ -305,31 +305,25 @@
     meta_in[...] = table
     meta[z, y] = table
 
-    @pl.when(me == 0)
-    def _():
-        halo[...] = jnp.zeros(halo.shape, bf16)
-
-    @pl.when(me > 0)
-    def _():
-        halo_copy().wait_recv()
-
-    joined = jnp.concatenate([halo[...], pool[...]], axis=0).astype(f32)
-    runs = [joined]
-    for by in (1, 2, 4, 8):
-        runs.append(runs[-1] + pltpu.roll(runs[-1], by, 0))
-    total = jnp.where(
-        tp == 0, runs[1], jnp.where(tp == 1, runs[2], jnp.where(tp == 2, runs[3], runs[4]))
-    )[reach:]
-    span = jnp.where(tp == 0, 2, jnp.where(tp == 1, 4, jnp.where(tp == 2, 8, 16)))
-    place = lax.broadcasted_iota(jnp.int32, (row_count, 1), 0) + me * row_count + 1
-    counted = jnp.minimum(place, span).astype(f32)
-    diff = (total / counted - joined[reach:]).astype(bf16)
-    pooled[...] = (
-        jnp.dot(diff, mix[...], preferred_element_type=f32) * gain[...]
-    ).astype(bf16)
-
-    def project(yy, cc):
-        span = pl.ds(block(yy, cc), tokens)
+    def pool_rows(joined, first_place):
+        runs = [joined.astype(f32)]
+        for by in (1, 2, 4, 8):
+            runs.append(runs[-1] + pltpu.roll(runs[-1], by, 0))
+        total = jnp.where(
+            tp == 0, runs[1], jnp.where(tp == 1, runs[2], jnp.where(tp == 2, runs[3], runs[4]))
+        )[reach:]
+        span = jnp.where(tp == 0, 2, jnp.where(tp == 1, 4, jnp.where(tp == 2, 8, 16)))
+        place = lax.broadcasted_iota(jnp.int32, (total.shape[0], 1), 0) + first_place + 1
+        counted = jnp.minimum(place, span).astype(f32)
+        diff = (total / counted - runs[0][reach:]).astype(bf16)
+        product = jnp.dot(diff, mix[...], preferred_element_type=f32)
+        return (product * gain[...]).astype(bf16)
+
+    early = jnp.zeros(halo.shape, bf16)
+    pooled[...] = pool_rows(jnp.concatenate([early, pool[...]], axis=0), me * row_count)
+
+    for yy, place in ((1 - y, 0), (y, 1)):
+        span = pl.ds(block(yy, 0), 2 * tokens)
 
         @pl.loop(0, front)
         def _(h):
@@ -337,21 +331,36 @@
                 pooled[span, :], proj[:, fcols(h)], preferred_element_type=f32
             ).astype(bf16)
 
-    for yy, place in ((1 - y, 0), (y, 1)):
-        project(yy, 1 - c)
-
-        @pl.loop(0, pieces)
+        @pl.loop(1, pieces)
         def _(k):
             pair_copy(yy, place, k).start()
 
-        project(yy, c)
+    @pl.when(me == 0)
+    def _():
+        halo[...] = jnp.zeros(halo.shape, bf16)
+
+    @pl.when(me > 0)
+    def _():
+        halo_copy().wait_recv()
+
+    late = pool_rows(jnp.concatenate([halo[...], pool[:reach, :]], axis=0), me * row_count)
+
+    @pl.loop(0, front)
+    def _(h):
+        part[:reach, fcols(h)] = jnp.dot(
+            late, proj[:, fcols(h)], preferred_element_type=f32
+        ).astype(bf16)
+
+    pair_copy(1 - y, 0, 0).start()
+    pair_copy(y, 1, 0).start()
 
     @pl.loop(1, 8)
     def _(q):
         meta_copy(q).start()
 
     @pl.loop(0, pieces)
-    def _(k):
+    def _(step):
+        k = (step + 1) % pieces
         pair_copy(1 - y, 0, k).wait_recv()
         far_out[piece(k)] = (
             part[block_piece(1 - y, c, k)].astype(f32) + pair_in[0, piece(k)].astype(f32)
@@ -359,7 +368,8 @@
         far_copy(k).start()
 
     @pl.loop(0, pieces)
-    def _(k):
+    def _(step):
+        k = (step + 1) % pieces
         pair_copy(y, 1, k).wait_recv()
         far_copy(k).wait_recv()
         added = (
@@ -401,7 +411,8 @@
         picks = picks_of(zt)
 
         @pl.loop(0, pieces)
-        def _(k):
+        def _(step):
+            k = (step + 1) % pieces
             pass_copy(zt, k, z1, ra_send).wait_recv()
             onward(k)
 
@@ -466,11 +477,6 @@
             parts[zt, spot(xx, y), bcols(h)] = total.astype(bf16)
         xb_copy(zt, False, h).start()
 
-    def far_sum(zt):
-        @pl.loop(0, back)
-        def _(h):
-            far_piece(zt, h)
-
     def weights_of(zt, yt):
         places = meta[zt, yt, :experts, :]
         shares = meta[zt, yt, experts:, :]
@@ -503,25 +509,26 @@
             sums[zt, 1 - y, :, bcols(h)] = blend(there, zt, 1 - y, h).astype(bf16)
             home_copy(zt, 1 - y, side, h).start()
 
-    def near_same(zt, side, first=0, stop=back):
-        here = weights_of(zt, y)
+    def near_same(first, stop):
+        here = weights_of(z1, y)
 
         @pl.loop(first, stop)
         def _(h):
-            total = blend(here, zt, y, h)
-
-            @pl.when(mid)
-            def _():
-                line_copy(zt, h, z1).wait_recv()
-                sums[zt, y, :, bcols(h)] = (
-                    total + line_in[zt, :, bcols(h)].astype(f32)
-                ).astype(bf16)
-
-            @pl.when(end)
-            def _():
-                sums[zt, y, :, bcols(h)] = total.astype(bf16)
-
-            home_copy(zt, y, side, h).start()
+            sums[z1, y, :, bcols(h)] = blend(here, z1, y, h).astype(bf16)
+            home_copy(z1, y, 0, h).start()
+
+    def merge_same():
+        here = weights_of(z2, y)
+
+        @pl.loop(0, back)
+        def _(h):
+            far_piece(z3, h)
+            total = blend(here, z2, y, h)
+            line_copy(z2, h, z1).wait_recv()
+            sums[z2, y, :, bcols(h)] = (
+                total + line_in[z2, :, bcols(h)].astype(f32)
+            ).astype(bf16)
+            home_copy(z2, y, 1, h).start()
 
     def far_back():
         mixes[0] = weights_of(z3, y)
@@ -630,9 +637,9 @@
     complete = scoped(complete, "complete")
     compute = scoped(compute, "compute")
     pair_sum = scoped(pair_sum, "pair_sum")
-    far_sum = scoped(far_sum, "far_sum")
     near_other = scoped(near_other, "near_other")
     near_same = scoped(near_same, "near_same")
+    merge_same = scoped(merge_same, "merge_same")
     far_back = scoped(far_back, "far_back")
     own_back = scoped(own_back, "own_back")
     last_send = scoped(last_send, "last_send")
@@ -652,61 +659,76 @@
     def _(h):
         gather(meta_picks, z, h)
 
+    arrive(z1, first_on)
+
+    @pl.when(mid)
+    def _():
+        arrive(z2, onto(z2, z1, ra_send))
+
+    turn(z1)
+
+    @pl.when(mid)
+    def _():
+        turn(z2)
+
     turn(z)
-    arrive(z1, first_on)
 
     @pl.when(mid)
     def _():
-        arrive(z2, onto(z2, z1, ra_send))
-
-    turn(z1)
-
-    @pl.when(mid)
-    def _():
-        turn(z2)
         arrive(z3, onto(z3, z1, ra_send))
 
-    complete(z)
+    @pl.when(end)
+    def _():
+        arrive(z2, nothing)
+
+    for load in loads:
+        load.wait()
+    complete(z1)
+    compute(z1)
     for zt in (z, z1, z2, z3):
         meta_here(zt, 1 - y)
-    for load in loads:
-        load.wait()
-    compute(z)
 
     @pl.when(end)
     def _():
-        arrive(z2, nothing)
-
-    complete(z1)
-    compute(z1)
-
-    @pl.when(end)
-    def _():
+        pair_sum(z1, False, 0, back // 2)
         turn(z2)
-        pair_sum(z1, False, 0, back // 2)
         arrive(z3, nothing)
         pair_sum(z1, False, back // 2, back)
         near_other(z1, 0, 0, back // 2)
+        near_same(0, back // 2)
 
     @pl.when(mid)
     def _():
         turn(z3)
         pair_sum(z1, False)
 
-    complete(z2)
-    compute(z2)
+    middle = ((z + 1) // 2) % 2
+    second = z + (z2 - z) * middle
+    third = z2 + (z - z2) * middle
+    complete(second)
+    compute(second)
 
     @pl.when(end)
     def _():
         turn(z3)
+
+    @pl.when(mid)
+    def _():
+        pair_sum(z2, False)
+
+    complete(third)
+    compute(third)
+
+    @pl.when(end)
+    def _():
+        near_other(z1, 0, back // 2, back)
+        near_same(back // 2, back)
         pair_sum(z2, True)
-        near_other(z1, 0, back // 2, back)
-        near_same(z1, 0)
         pair_sum(z, False)
 
     @pl.when(mid)
     def _():
-        pair_sum(z2, False)
+        near_other(z1, 0)
 
     complete(z3)
     compute(z3)
@@ -715,18 +737,18 @@
     @pl.when(end)
     def _():
         far_chain()
-        own_back()
-        last_send()
 
     @pl.when(mid)
     def _():
         pair_sum(z, False)
-        near_other(z1, 0)
         near_other(z2, 1)
-        far_sum(z3)
-        own_back()
-        last_send()
-        near_same(z2, 1)
+        merge_same()
+
+    own_back()
+    last_send()
+
+    @pl.when(mid)
+    def _():
         far_back()
 
     with jax.named_scope("finish"):
@@ -778,7 +800,7 @@
         line_copy(z2, None, z1).wait_send()
 
 
-FRONT, BACK, LAG = 4, 4, 2
+FRONT, BACK, LAG = 4, 8, 3
 
 
 def layer_kernel(

time: 129 us -> 122 us (0.946)
  Pallas kernels: 127 us -> 119 us
    pallas_call x1, Pallas kernels: 127 us -> 119 us  [layer_kernel(): pl.pallas_call(functools.partial(moe_kernel, FRONT, BACK, capacity, exper...]
where the time goes in v4:
time: 122 us; the launch traced here: 121 us
  Pallas kernels  119 us (98%)
  local copies, waits for them, and re-layouts  1.87 us (2%)
    pallas_call x1, Pallas kernels, layer_kernel(): pl.pallas_call(functools.partial(moe_kernel, FRONT, BACK, capacity, exper...  119 us

profile of v4, /device:TPU:0, one launch (start us, length us, event | category | flops | bytes accessed | tf_op | source)
XLA Modules:
  0.0 121.4 jit_solution(6342949000194337865)
XLA Ops:
  0.0 119.5 %moe_exchange.1 = bf16[64,4096]{1,0:T(8,128)(2,1)} custom-call(bf16[256,4096]{1,0:T(8,128)(2,1)} %resid.1, bf16[256,256]{1,0:T(8,128)(2,1)} %pool_in.1, bf16[1,256,256]{2,1,0:T(8,128)(2,1)} %pool_mix.1, f32[1,256]{1,0:T(1,128)} %bitcast.7, bf16[256,4096]{1,0:T(8,128)(2,1)} %out_proj.1, f32[1,4096]{1,0:T(1,128)} %bitcast.4, bf16[1,4096,256]{2,1,0:T(8,128)(2,1)} %wg_hbm.1, ...), custom_call_target="tpu_custom_call" | custom-call | flops 6442450944 | bytes 8388608 | tf_op jit(solution)/shard_map/moe_exchange/pallas_call | solution.py:823
  119.5 1.9 %copy.13 = bf16[64,4096]{1,0:T(8,128)(2,1)} copy(bf16[64,4096]{1,0:T(8,128)(2,1)} %moe_exchange.1) | data formatting | bytes 1048576

commit v5 on v4

--- a/solution.py
+++ b/solution.py
@@ -710,6 +710,7 @@
 
     @pl.when(end)
     def _():
+        pair_sum(z, False)
         turn(z3)
 
     @pl.when(mid)
@@ -724,7 +725,6 @@
         near_other(z1, 0, back // 2, back)
         near_same(back // 2, back)
         pair_sum(z2, True)
-        pair_sum(z, False)
 
     @pl.when(mid)
     def _():
@@ -750,9 +750,6 @@
     @pl.when(mid)
     def _():
         far_back()
-
-    with jax.named_scope("finish"):
-        finish()
 
     @pl.loop(1, 8)
     def _(q):
@@ -777,10 +774,6 @@
     xb_copy(z3, False, None).wait_send()
     yb_copy(z3, 0, None).wait_send()
     yb_copy(z3, 1, None).wait_send()
-    line_copy(z3, None, z1).wait_send()
-    home_copy(z1, 0, 0, None).wait_send()
-    home_copy(z1, 1, 0, None).wait_send()
-    last_copy(None).wait_send()
 
     @pl.when(mid)
     def _():
@@ -799,8 +792,16 @@
         yb_copy(z2, 1, None).wait_send()
         line_copy(z2, None, z1).wait_send()
 
-
-FRONT, BACK, LAG = 4, 8, 3
+    with jax.named_scope("finish"):
+        finish()
+
+    line_copy(z3, None, z1).wait_send()
+    home_copy(z1, 0, 0, None).wait_send()
+    home_copy(z1, 1, 0, None).wait_send()
+    last_copy(None).wait_send()
+
+
+FRONT, BACK, LAG = 4, 4, 2
 
 
 def layer_kernel(

time: 122 us -> 120 us (0.984)
  Pallas kernels: 119 us -> 117 us
    pallas_call x1, Pallas kernels: 119 us -> 117 us  [layer_kernel(): pl.pallas_call(functools.partial(moe_kernel, FRONT, BACK, capacity, exper...]
where the time goes in v5:
time: 120 us; the launch traced here: 119 us
  Pallas kernels  117 us (98%)
  local copies, waits for them, and re-layouts  1.87 us (2%)
    pallas_call x1, Pallas kernels, layer_kernel(): pl.pallas_call(functools.partial(moe_kernel, FRONT, BACK, capacity, exper...  117 us

profile of v5, /device:TPU:0, one launch (start us, length us, event | category | flops | bytes accessed | tf_op | source)
XLA Modules:
  0.0 119.4 jit_solution(15976855365345837381)
XLA Ops:
  0.0 117.5 %moe_exchange.1 = bf16[64,4096]{1,0:T(8,128)(2,1)} custom-call(bf16[256,4096]{1,0:T(8,128)(2,1)} %resid.1, bf16[256,256]{1,0:T(8,128)(2,1)} %pool_in.1, bf16[1,256,256]{2,1,0:T(8,128)(2,1)} %pool_mix.1, f32[1,256]{1,0:T(1,128)} %bitcast.7, bf16[256,4096]{1,0:T(8,128)(2,1)} %out_proj.1, f32[1,4096]{1,0:T(1,128)} %bitcast.4, bf16[1,4096,256]{2,1,0:T(8,128)(2,1)} %wg_hbm.1, ...), custom_call_target="tpu_custom_call" | custom-call | flops 6442450944 | bytes 8388608 | tf_op jit(solution)/shard_map/moe_exchange/pallas_call | solution.py:824
  117.5 1.9 %copy.13 = bf16[64,4096]{1,0:T(8,128)(2,1)} copy(bf16[64,4096]{1,0:T(8,128)(2,1)} %moe_exchange.1) | data formatting | bytes 1048576
